TPU v7x, 32 devices: a whole 2x2x4 slice. The times are simulated.
32 devices in a mesh: grp: 2 (over y), sp: 4 (over z), tp: 4 (over x, core).
Axes of the slice: x: 2, y: 2, z: 4, core: 2. Of those that a mesh axis runs over, the one named last changes fastest.
Arguments:
- latent: bfloat16 [2048, 512], P(('grp', 'sp')), parts along dimension 0, may hold values from -6 to 6
- rope_key: bfloat16 [2048, 64], P(('grp', 'sp')), parts along dimension 0, may hold values from -6 to 6
- wide_query: bfloat16 [2048, 1536], P(('grp', 'sp'), 'tp'), parts along dimension 0, may hold values from -1300 to 1300
- narrow_query: bfloat16 [2048, 1024], P(('grp', 'sp'), 'tp'), parts along dimension 0, may hold values from -1300 to 1300
- wide_key_weight: bfloat16 [512, 1024], P(None, 'tp'), may hold values from -0.25 to 0.25
- wide_value_weight: bfloat16 [512, 1024], P(None, 'tp'), may hold values from -0.25 to 0.25
- narrow_key_weight: bfloat16 [512, 512], P(None, 'tp'), may hold values from -0.25 to 0.25
- narrow_value_weight: bfloat16 [512, 512], P(None, 'tp'), may hold values from -0.25 to 0.25
- latent_norm_scale: float32 [512], replicated, may hold values from 0.1 to 1.9
- out_wide: bfloat16 [1024, 4096], P('tp'), may hold values from -0.4375 to 0.4375
- out_narrow: bfloat16 [512, 4096], P('tp'), may hold values from -0.4375 to 0.4375
- residual: bfloat16 [2048, 4096], P(('grp', 'sp', 'tp')), parts along dimension 0, may hold values from -6 to 6
- ffn_gain: float32 [4096], replicated, may hold values from 0.1 to 1.9
- shared_gate: bfloat16 [4096, 512], P(None, 'tp'), may hold values from -0.09375 to 0.09375
- shared_up: bfloat16 [4096, 512], P(None, 'tp'), may hold values from -0.09375 to 0.09375
- shared_down: bfloat16 [512, 4096], P('tp'), may hold values from -0.25 to 0.25
- expert_gate: bfloat16 [16, 4096, 192], P(('sp', 'tp')), may hold values from -0.09375 to 0.09375
- expert_up: bfloat16 [16, 4096, 192], P(('sp', 'tp')), may hold values from -0.09375 to 0.09375
- expert_down: bfloat16 [16, 192, 4096], P(('sp', 'tp')), may hold values from -0.4375 to 0.4375
- routes: int32 [2048, 2], P(('grp', 'sp', 'tp')), parts along dimension 0, may hold values from 0 to 15, all different within a row; in each aligned block of 64 rows (0 to 63, 64 to 127, ...) at most 16 rows name the same one
- route_weights: float32 [2048, 2], P(('grp', 'sp', 'tp')), parts along dimension 0, may hold values from 0.25 to 1.5
Outputs:
- layer_out: bfloat16 [2048, 4096], P(('grp', 'sp', 'tp')), parts along dimension 0
There are 2 independent parts, one for each index of `grp`. A program takes and returns all parts, laid end to end along the dimension named above; an argument that names none is the same for every part. Nothing has to cross between parts.
Inputs may be any that keep to these rules, and one draw needn't show every extreme that they name: `routes`: each row names 2 different experts; in each aligned block of 64 rows no expert is named by more than 16 rows, and some block has an expert named exactly 16 times.
All inputs are finite; a program needn't handle non-finite values.
Results may differ from a plain program's by a relative error of at most 0.023.
Values may be sent and summed in bfloat16 or wider, within the bound.
A program may use at most 128 MiB of HBM per device.

v0:
```python
import jax
import jax.numpy as jnp
from jax import lax
from jax.experimental import pallas as pl
from jax.experimental.pallas import tpu as pltpu
from jax.sharding import PartitionSpec as P

ROPE = 64
WIDE_HEAD_SIZE = 128
NARROW_HEAD_SIZE = 64


MESH = pl.DeviceIdType.MESH
VMEM = pl.BlockSpec(memory_space=pltpu.VMEM)


def flip(index, bits):
    mask = 1
    while mask <= bits:
        if bits & mask:
            index = index + mask - 2 * mask * ((index // mask) % 2)
        mask *= 2
    return index


def masks_of(count):
    return [1 << k for k in range(count.bit_length() - 1)]


def low_bit(number):
    return number & -number


def greet(partners):
    barrier = pltpu.get_barrier_semaphore()
    for partner in partners:
        pl.semaphore_signal(barrier, inc=1, device_id=partner, device_id_type=MESH)
    pl.semaphore_wait(barrier, len(partners))


def doubling_order(count):
    return sorted(range(count), key=lambda d: (bin(d).count("1"), -d))


def remote(src, dst, send_sem, recv_sem, target):
    return pltpu.make_async_remote_copy(
        src_ref=src,
        dst_ref=dst,
        send_sem=send_sem,
        recv_sem=recv_sem,
        device_id=target,
        device_id_type=MESH,
    )


def spread_kernel(n_sp, n_tp, x_ref, out_ref, z_send, z_recv, t_send, t_recv, own_sem):
    sp, tp = lax.axis_index("sp"), lax.axis_index("tp")
    tok = x_ref.shape[0]
    part = tok // n_tp
    targets = [{"sp": lax.rem(sp + r, n_sp)} for r in range(1, n_sp)]
    greet(targets + [{"tp": flip(tp, m)} for m in masks_of(n_tp)])

    def rows(block, member):
        return pl.ds(pl.multiple_of(block * tok + member * part, part), part)

    own = pltpu.make_async_copy(
        x_ref, out_ref.at[pl.ds(pl.multiple_of(sp * tok, tok), tok)], own_sem
    )
    sends = []
    for r in range(1, n_sp):
        copy = remote(
            x_ref.at[pl.ds(pl.multiple_of(tp * part, part), part)],
            out_ref.at[rows(sp, tp)],
            z_send.at[r],
            z_recv.at[r],
            targets[r - 1],
        )
        copy.start()
        sends.append(copy)
    own.start()

    def piece(r, d):
        return out_ref.at[rows(lax.rem(sp + n_sp - r, n_sp), flip(tp, d))]

    for d in doubling_order(n_tp):
        for r in range(1, n_sp):
            block = piece(r, d)
            if d == 0:
                sends[r - 1].wait_recv()
            else:
                remote(
                    block, block, t_send.at[r, d], t_recv.at[r, d], {"tp": flip(tp, low_bit(d))}
                ).wait_recv()
            for mask in reversed(masks_of(low_bit(d) if d else n_tp)):
                copy = remote(
                    block,
                    block,
                    t_send.at[r, d + mask],
                    t_recv.at[r, d + mask],
                    {"tp": flip(tp, mask)},
                )
                copy.start()
                sends.append(copy)
    for copy in sends:
        copy.wait_send()
    own.wait()


def spread(x, n_sp, n_tp):
    tok, width = x.shape
    return pl.pallas_call(
        lambda *refs: spread_kernel(n_sp, n_tp, *refs),
        out_shape=jax.ShapeDtypeStruct((n_sp * tok, width), x.dtype),
        in_specs=[VMEM],
        out_specs=VMEM,
        scratch_shapes=[
            pltpu.SemaphoreType.DMA((n_sp,)),
            pltpu.SemaphoreType.DMA((n_sp,)),
            pltpu.SemaphoreType.DMA((n_sp, n_tp)),
            pltpu.SemaphoreType.DMA((n_sp, n_tp)),
            pltpu.SemaphoreType.DMA,
        ],
        compiler_params=pltpu.CompilerParams(collective_id=0, has_side_effects=True),
        cost_estimate=pl.CostEstimate(flops=0, bytes_accessed=30_000_000, transcendentals=0),
    )(x)


def gather_kernel(
    n_tp, pieces, x_ref, blocks_ref, out_ref, moved_ref, send, recv, own_sem, *semaphores
):
    exchange = Exchange(blocks_ref, moved_ref, *semaphores)
    tp = lax.axis_index("tp")
    rows, width = x_ref.shape
    part = width // pieces
    exchange.greet()

    def block(d, c):
        start = pl.multiple_of(flip(tp, d) * rows, rows)
        return out_ref.at[pl.ds(start, rows), pl.ds(c * part, part)]

    own = pltpu.make_async_copy(
        x_ref, out_ref.at[pl.ds(pl.multiple_of(tp * rows, rows), rows)], own_sem
    )
    sends = []
    for d in doubling_order(n_tp):
        for c in range(pieces):
            source = x_ref.at[:, pl.ds(c * part, part)] if d == 0 else block(d, c)
            if d:
                remote(
                    source, source, send.at[d, c], recv.at[d, c], {"tp": flip(tp, low_bit(d))}
                ).wait_recv()
            for mask in reversed(masks_of(low_bit(d) if d else n_tp)):
                copy = remote(
                    source,
                    block(d, c),
                    send.at[d + mask, c],
                    recv.at[d + mask, c],
                    {"tp": flip(tp, mask)},
                )
                copy.start()
                sends.append(copy)
        if d == 0:
            exchange.start()
            own.start()
    for copy in sends:
        copy.wait_send()
    own.wait()
    exchange.finish()


def gather_rows(x, blocks, n_tp, pieces=2):
    rows, width = x.shape
    return pl.pallas_call(
        lambda *refs: gather_kernel(n_tp, pieces, *refs),
        out_shape=[
            jax.ShapeDtypeStruct((n_tp * rows, width), x.dtype),
            jax.ShapeDtypeStruct(blocks.shape, blocks.dtype),
        ],
        in_specs=[VMEM] * 2,
        out_specs=[VMEM] * 2,
        scratch_shapes=[
            pltpu.SemaphoreType.DMA((n_tp, pieces)),
            pltpu.SemaphoreType.DMA((n_tp, pieces)),
            pltpu.SemaphoreType.DMA,
        ]
        + exchange_semaphores(blocks.shape[0]),
        compiler_params=pltpu.CompilerParams(collective_id=1, has_side_effects=True),
        cost_estimate=pl.CostEstimate(flops=0, bytes_accessed=40_000_000, transcendentals=0),
    )(x, blocks)


def scatter_kernel(n_tp, pieces, pairs, moving, *refs):
    lefts, rights = refs[:pairs], refs[pairs : 2 * pairs]
    refs = refs[2 * pairs :]
    exchange = None
    if moving:
        blocks_ref, out_ref, moved_ref, sent, got, send, recv = refs[:7]
        exchange = Exchange(blocks_ref, moved_ref, *refs[7:])
    else:
        out_ref, sent, got, send, recv = refs
    tp = lax.axis_index("tp")
    rows, width = out_ref.shape
    part = width // pieces
    if moving:
        exchange.greet()
        exchange.start()
    else:
        greet([{"tp": flip(tp, m)} for m in masks_of(n_tp)])
    copies = {}

    def product(d, c):
        start = pl.multiple_of(flip(tp, d) * rows, rows)
        total = None
        for left, right in zip(lefts, rights):
            term = jnp.dot(
                left[pl.ds(start, rows), :],
                right[:, pl.ds(c * part, part)],
                preferred_element_type=jnp.float32,
            )
            total = term if total is None else total + term
        return total

    def summed(d, c, below):
        total = product(d, c)
        if below > 1:
            total = total.astype(jnp.bfloat16).astype(jnp.float32)
        for mask in masks_of(below):
            copies[d + mask, c].wait_recv()
            total = total + got[d + mask, :, pl.ds(c * part, part)].astype(jnp.float32)
        return total

    def pass_on(mask, c):
        for d in range(mask, n_tp, 2 * mask):
            sent[d, :, pl.ds(c * part, part)] = summed(d, c, mask).astype(jnp.bfloat16)
            copies[d, c] = remote(
                sent.at[d, :, pl.ds(c * part, part)],
                got.at[d, :, pl.ds(c * part, part)],
                send.at[d, c],
                recv.at[d, c],
                {"tp": flip(tp, mask)},
            )
            copies[d, c].start()

    masks = masks_of(n_tp)
    for step in range(pieces + len(masks) - 1):
        for stage, mask in enumerate(masks):
            if 0 <= step - stage < pieces:
                pass_on(mask, step - stage)
    for c in range(pieces):
        out_ref[:, pl.ds(c * part, part)] = summed(0, c, n_tp)
    for copy in copies.values():
        copy.wait_send()
    if moving:
        exchange.finish()


def dot_scatter(lefts, rights, n_tp, collective, blocks=None, pieces=4):
    rows, width = lefts[0].shape[0] // n_tp, rights[0].shape[1]
    pairs, moving = len(lefts), blocks is not None
    shapes = [jax.ShapeDtypeStruct((rows, width), jnp.float32)]
    operands = (*lefts, *rights)
    scratch = [
        pltpu.VMEM((n_tp, rows, width), jnp.bfloat16),
        pltpu.VMEM((n_tp, rows, width), jnp.bfloat16),
        pltpu.SemaphoreType.DMA((n_tp, pieces)),
        pltpu.SemaphoreType.DMA((n_tp, pieces)),
    ]
    if moving:
        shapes.append(jax.ShapeDtypeStruct(blocks.shape, blocks.dtype))
        operands += (blocks,)
        scratch += exchange_semaphores(blocks.shape[0])
    return pl.pallas_call(
        lambda *refs: scatter_kernel(n_tp, pieces, pairs, moving, *refs),
        out_shape=shapes,
        in_specs=[VMEM] * len(operands),
        out_specs=[VMEM] * len(shapes),
        scratch_shapes=scratch,
        compiler_params=pltpu.CompilerParams(collective_id=collective, has_side_effects=True),
        cost_estimate=pl.CostEstimate(flops=0, bytes_accessed=40_000_000, transcendentals=0),
    )(*operands)


EPS = 1e-06
ROPE_BASE = 10000.0
NEG_FILL = -1e30


def attend_kernel(sizes, packed, cosine, sine, *refs):
    groups = len(sizes)
    queries, key_ws, value_ws = refs[:groups], refs[groups : 2 * groups], refs[2 * groups : 3 * groups]
    outs = refs[3 * groups : 4 * groups]
    scratch = refs[4 * groups :]
    sp = lax.axis_index("sp")
    tok = cosine.shape[0]
    latent_width = key_ws[0].shape[0]
    lanes = packed.shape[1] - latent_width
    half = ROPE // 2

    def grid(shape):
        return lax.broadcasted_iota(jnp.int32, shape, 0), lax.broadcasted_iota(jnp.int32, shape, 1)

    for g, size in enumerate(sizes):
        plain, turned, peak, total, mixed = scratch[5 * g : 5 * g + 5]
        query = queries[g][...]
        width = query.shape[1]
        for h in range(plain.shape[0]):
            i, j = grid((width, key_ws[g].shape[1]))
            select = (i == j + h * ROPE) & (j >= h * size) & (j < (h + 1) * size)
            plain[h] = jnp.dot(
                query, select.astype(jnp.bfloat16), preferred_element_type=jnp.float32
            ).astype(jnp.bfloat16)
            i, j = grid((width, lanes))
            base = h * (size + ROPE) + size
            same = ((i == j + base) & (j < ROPE)).astype(jnp.float32)
            upper = ((i == j + base + half) & (j < half)).astype(jnp.float32)
            lower = ((i == j + base - half) & (j >= half) & (j < ROPE)).astype(jnp.float32)
            straight = jnp.dot(
                query, same.astype(jnp.bfloat16), preferred_element_type=jnp.float32
            )
            crossed = jnp.dot(
                query, (lower - upper).astype(jnp.bfloat16), preferred_element_type=jnp.float32
            )
            turned[h] = (straight * cosine[...] + crossed * sine[...]).astype(jnp.bfloat16)
        peak[...] = jnp.full_like(peak, NEG_FILL)
        total[...] = jnp.zeros_like(total)
        mixed[...] = jnp.zeros_like(mixed)

    def one_block(index, carry):
        start = pl.ds(pl.multiple_of(index * tok, tok), tok)
        latent = packed[start, :latent_width]
        turned_rows = packed[start, latent_width:]
        i, j = grid((tok, tok))
        visible = index * tok + j <= sp * tok + i
        across = (((1,), (1,)), ((), ()))
        for g, size in enumerate(sizes):
            plain, turned, peak, total, mixed = scratch[5 * g : 5 * g + 5]
            factor = (size + ROPE) ** (-0.5)
            keys = jnp.dot(latent, key_ws[g][...], preferred_element_type=jnp.float32)
            keys = keys.astype(jnp.bfloat16)
            values = jnp.dot(latent, value_ws[g][...], preferred_element_type=jnp.float32)
            values = values.astype(jnp.bfloat16)
            for h in range(plain.shape[0]):
                scores = lax.dot_general(
                    plain[h], keys, across, preferred_element_type=jnp.float32
                ) + lax.dot_general(
                    turned[h], turned_rows, across, preferred_element_type=jnp.float32
                )
                scores = jnp.where(visible, scores * factor, NEG_FILL)
                old = peak[h]
                new = jnp.maximum(old, jnp.max(scores, axis=1, keepdims=True))
                probs = jnp.where(visible, jnp.exp(scores - new), 0.0)
                fading = jnp.exp(old - new)
                peak[h] = new
                total[h] = total[h] * fading + jnp.sum(probs, axis=1, keepdims=True)
                mixed[h] = mixed[h] * fading + jnp.dot(
                    probs.astype(jnp.bfloat16), values, preferred_element_type=jnp.float32
                )
        return carry

    lax.fori_loop(0, sp + 1, one_block, 0)
    for g, size in enumerate(sizes):
        plain, turned, peak, total, mixed = scratch[5 * g : 5 * g + 5]
        i, j = grid(outs[g].shape)
        result = jnp.zeros(outs[g].shape, jnp.float32)
        for h in range(plain.shape[0]):
            own = (j >= h * size) & (j < (h + 1) * size)
            result = jnp.where(own, mixed[h] / total[h], result)
        outs[g][...] = result.astype(jnp.bfloat16)


def attend(packed, cosine, sine, queries, key_ws, value_ws, sizes):
    tok, lanes = cosine.shape
    scratch = []
    for g, size in enumerate(sizes):
        heads = value_ws[g].shape[1] // size
        scratch += [
            pltpu.VMEM((heads, tok, key_ws[g].shape[1]), jnp.bfloat16),
            pltpu.VMEM((heads, tok, lanes), jnp.bfloat16),
            pltpu.VMEM((heads, tok, 1), jnp.float32),
            pltpu.VMEM((heads, tok, 1), jnp.float32),
            pltpu.VMEM((heads, tok, value_ws[g].shape[1]), jnp.float32),
        ]
    return pl.pallas_call(
        lambda *refs: attend_kernel(sizes, *refs),
        out_shape=[jax.ShapeDtypeStruct((tok, w.shape[1]), jnp.bfloat16) for w in value_ws],
        in_specs=[VMEM] * (3 + 3 * len(sizes)),
        out_specs=[VMEM] * len(sizes),
        scratch_shapes=scratch,
    )(packed, cosine, sine, *queries, *key_ws, *value_ws)


class Exchange:
    def __init__(self, source, dest, send, recv, own_sem):
        self.refs = source, dest, send, recv
        self.sp, self.tp = lax.axis_index("sp"), lax.axis_index("tp")
        self.n_sp, self.n_tp = lax.axis_size("sp"), lax.axis_size("tp")
        self.count = self.n_sp * self.n_tp
        self.me = self.sp * self.n_tp + self.tp
        self.own = pltpu.make_async_copy(source.at[self.me], dest.at[self.me], own_sem)

    def target(self, k):
        return (
            lax.rem(self.sp + k // self.n_tp, self.n_sp),
            lax.rem(self.tp + lax.rem(k, self.n_tp), self.n_tp),
        )

    def greet(self):
        barrier = pltpu.get_barrier_semaphore()

        def one(k, carry):
            sp, tp = self.target(k)
            pl.semaphore_signal(
                barrier, inc=1, device_id={"sp": sp, "tp": tp}, device_id_type=MESH
            )
            return carry

        lax.fori_loop(1, self.count, one, 0)
        pl.semaphore_wait(barrier, self.count - 1)

    def copy(self, k):
        source, dest, send, recv = self.refs
        sp, tp = self.target(k)
        return remote(
            source.at[sp * self.n_tp + tp],
            dest.at[self.me],
            send.at[k],
            recv.at[k],
            {"sp": sp, "tp": tp},
        )

    def start(self):
        def one(k, carry):
            self.copy(self.count - k).start()
            return carry

        lax.fori_loop(1, self.count, one, 0)
        self.own.start()

    def finish(self):
        def one(k, carry):
            self.copy(k).wait()
            return carry

        lax.fori_loop(1, self.count, one, 0)
        self.own.wait()


def exchange_semaphores(count):
    return [
        pltpu.SemaphoreType.DMA((count,)),
        pltpu.SemaphoreType.DMA((count,)),
        pltpu.SemaphoreType.DMA,
    ]


def rms_scale(values, gain):
    return values * lax.rsqrt(jnp.mean(values * values, axis=-1, keepdims=True) + EPS) * gain


def body(
    latent,
    rope_key,
    wide_query,
    narrow_query,
    wide_key_weight,
    wide_value_weight,
    narrow_key_weight,
    narrow_value_weight,
    latent_norm_scale,
    out_wide,
    out_narrow,
    residual,
    ffn_gain,
    shared_gate,
    shared_up,
    shared_down,
    expert_gate,
    expert_up,
    expert_down,
    routes,
    route_weights,
):
    tok_dev = latent.shape[0]
    seq_index = lax.axis_index("sp")
    own_pos = seq_index * tok_dev + jnp.arange(tok_dev, dtype=jnp.int32)
    n_sp, n_tp = lax.axis_size("sp"), lax.axis_size("tp")
    normed_latent = rms_scale(latent.astype(jnp.float32), latent_norm_scale).astype(jnp.bfloat16)
    half = ROPE // 2
    lane = jnp.arange(ROPE + -ROPE % 128, dtype=jnp.int32)
    inverse = ROPE_BASE ** (-(lane % half).astype(jnp.float32) * 2.0 / ROPE)
    angles = own_pos.astype(jnp.float32)[:, None] * inverse[None, :]
    cosine, sine = jnp.cos(angles), jnp.sin(angles)
    row = jnp.arange(ROPE, dtype=jnp.int32)[:, None]
    same = (row == lane[None, :]).astype(jnp.bfloat16)
    cross = (row == lane[None, :] - half).astype(jnp.bfloat16) * (lane < ROPE)[None, :] - (
        (row == lane[None, :] + half) & (lane < half)[None, :]
    ).astype(jnp.bfloat16)
    turned_key = (
        jnp.dot(rope_key, same, preferred_element_type=jnp.float32) * cosine
        + jnp.dot(rope_key, cross.astype(jnp.bfloat16), preferred_element_type=jnp.float32) * sine
    ).astype(jnp.bfloat16)
    packed = spread(jnp.concatenate([normed_latent, turned_key], axis=1), n_sp, n_tp)
    wide_mix, narrow_mix = attend(
        packed,
        cosine,
        sine,
        (wide_query, narrow_query),
        (wide_key_weight, narrow_key_weight),
        (wide_value_weight, narrow_value_weight),
        (WIDE_HEAD_SIZE, NARROW_HEAD_SIZE),
    )
    (projected,) = dot_scatter((wide_mix, narrow_mix), (out_wide, out_narrow), n_tp, 2)
    stream = (residual.astype(jnp.float32) + projected).astype(jnp.bfloat16)
    normed = rms_scale(stream.astype(jnp.float32), ffn_gain).astype(jnp.bfloat16)
    rows_here, top_count = routes.shape
    local_experts = expert_gate.shape[0]
    experts_all = local_experts * lax.axis_size(("sp", "tp"))
    capacity = max(2, 2 * top_count * rows_here // experts_all)
    model_width = normed.shape[1]
    flat_routes = routes.reshape(-1)
    assigned = flat_routes.shape[0]
    choose = (flat_routes[:, None] == jnp.arange(experts_all, dtype=jnp.int32)[None, :]).astype(
        jnp.float32
    )
    lower_mask = (jnp.arange(assigned)[:, None] > jnp.arange(assigned)[None, :]).astype(jnp.float32)
    earlier = jnp.dot(lower_mask, choose, precision=lax.Precision.HIGHEST)
    slots = jnp.sum(earlier * choose, axis=1).astype(jnp.int32)
    target = flat_routes * capacity + slots
    send_map = jnp.any(
        target.reshape(rows_here, top_count)[None, :, :]
        == jnp.arange(experts_all * capacity, dtype=jnp.int32)[:, None, None],
        axis=2,
    ).astype(jnp.bfloat16)
    outgoing = jnp.dot(send_map, normed, preferred_element_type=jnp.float32).astype(jnp.bfloat16)
    devices = n_sp * n_tp
    outgoing = outgoing.reshape(devices, local_experts * capacity, model_width)
    piece, incoming = gather_rows(normed, outgoing, n_tp)
    sources = devices
    incoming = incoming.reshape(experts_all, capacity, model_width)
    grouped = incoming.reshape(sources, local_experts, incoming.shape[1], model_width)
    gate_part = jnp.einsum(
        "sxcd,xdf->sxcf", grouped, expert_gate, preferred_element_type=jnp.float32
    )
    up_part = jnp.einsum("sxcd,xdf->sxcf", grouped, expert_up, preferred_element_type=jnp.float32)
    active = (jax.nn.silu(gate_part) * up_part).astype(jnp.bfloat16)
    finished = jnp.einsum(
        "sxcf,xfd->sxcd", active, expert_down, preferred_element_type=jnp.float32
    ).astype(jnp.bfloat16)
    gate_part = jnp.dot(piece, shared_gate, preferred_element_type=jnp.float32)
    up_part = jnp.dot(piece, shared_up, preferred_element_type=jnp.float32)
    active = (jax.nn.silu(gate_part) * up_part).astype(jnp.bfloat16)
    shared, returned = dot_scatter(
        (active,), (shared_down,), n_tp, 3, finished.reshape(outgoing.shape)
    )
    slot_rows = returned.reshape(experts_all * capacity, model_width)
    by_choice = target.reshape(rows_here, top_count)
    routed = jnp.zeros((rows_here, model_width), jnp.float32)
    for choice in range(top_count):
        hot = by_choice[:, choice : choice + 1] == jnp.arange(experts_all * capacity)[None, :]
        picked = jnp.dot(
            hot.astype(jnp.bfloat16), slot_rows, preferred_element_type=jnp.float32
        )
        routed = routed + picked * route_weights[:, choice : choice + 1]
    return (stream.astype(jnp.float32) + shared + routed).astype(jnp.bfloat16)


def solution(mesh):
    placed = (
        P(("grp", "sp"), None),
        P(("grp", "sp"), None),
        P(("grp", "sp"), "tp"),
        P(("grp", "sp"), "tp"),
        P(None, "tp"),
        P(None, "tp"),
        P(None, "tp"),
        P(None, "tp"),
        P(),
        P("tp", None),
        P("tp", None),
        P(("grp", "sp", "tp"), None),
        P(),
        P(None, "tp"),
        P(None, "tp"),
        P("tp", None),
        P(("sp", "tp"), None, None),
        P(("sp", "tp"), None, None),
        P(("sp", "tp"), None, None),
        P(("grp", "sp", "tp"), None),
        P(("grp", "sp", "tp"), None),
    )
    return jax.shard_map(
        body, mesh=mesh, in_specs=placed, out_specs=P(("grp", "sp", "tp"), None), check_vma=False
    )
```

profile of v0, /device:TPU:0, one launch (start us, length us, event | category | flops | bytes accessed | tf_op | source)
XLA Modules:
  0.0 188.5 jit_solution(10074779783587421280)
XLA Ops:
  0.0 1.4 fusion.25
  1.4 1.3 fusion.27
  2.7 1.1 fusion.34
  3.8 1.1 fusion.36
  4.9 0.8 pad_maximum_fusion.refs_0_
  5.7 20.1 %shard_map.199.refs_0_ = bf16[1024,640]{1,0:T(8,128)(2,1)} custom-call(bf16[256,640]{1,0:T(8,128)(2,1)} %pad_maximum_fusion.refs_0_), custom_call_target="tpu_custom_call" | custom-call | bytes 30000000 | tf_op jit(solution)/shard_map/pallas_call | solution.py:111
  25.8 1.2 multiply_sine_fusion
  27.0 5.9 %shard_map.200 = (bf16[256,256]{1,0:T(8,128)(2,1)}, bf16[256,128]{1,0:T(8,128)(2,1)}) custom-call(bf16[1024,640]{1,0:T(8,128)(2,1)} %shard_map.199.refs_0_, f32[256,128]{1,0:T(8,128)} %get-tuple-element.20.refs_1_, f32[256,128]{1,0:T(8,128)} %get-tuple-element.19.refs_2_, bf16[256,384]{1,0:T(8,128)(2,1)} %refs_3_.2, bf16[256,256]{1,0:T(8,128)(2,1)} %refs_4_.1, ...), custom_call_target="tpu_custom_call" | custom-call | tf_op jit(solution)/shard_map/pallas_call | solution.py:383
  32.9 19.3 %shard_map.201 = f32[64,4096]{1,0:T(8,128)} custom-call(bf16[256,256]{1,0:T(8,128)(2,1)} %get-tuple-element.11.refs_0_, bf16[256,128]{1,0:T(8,128)(2,1)} %get-tuple-element.12.refs_1_, bf16[256,4096]{1,0:T(8,128)(2,1)} %refs_2_.1, bf16[128,4096]{1,0:T(8,128)(2,1)} %refs_3_.3), custom_call_target="tpu_custom_call" | custom-call | bytes 40000000 | tf_op jit(solution)/shard_map/pallas_call | solution.py:272
  52.3 1.5 fusion.31
  53.8 0.2 fusion.33.refs_0_
  54.1 0.1 eq.105
  54.3 0.2 fusion.28
  54.4 0.1 convert_element_type.93
  54.8 2.1 %convolution_convert_fusion.1 = bf16[256,4096]{1,0:T(8,128)(2,1)} fusion(pred[256,64]{0,1:T(8,128)(4,1)S(1)} %fusion.43, bf16[64,4096]{1,0:T(8,128)(2,1)S(1)} %fusion.33.refs_0_), kind=kOutput, calls=%fused_computation.1 | convolution fusion | flops 135266304 | bytes 2637824 | tf_op jit(solution)/shard_map/dot_general | solution.py:534
  56.9 61.2 %shard_map.202 = (bf16[256,4096]{1,0:T(8,128)(2,1)}, bf16[16,16,4096]{2,1,0:T(8,128)(2,1)}) custom-call(bf16[64,4096]{1,0:T(8,128)(2,1)} %copy-done.2, bf16[16,16,4096]{2,1,0:T(8,128)(2,1)} %bitcast.82), custom_call_target="tpu_custom_call" | custom-call | bytes 40000000 | tf_op jit(solution)/shard_map/pallas_call | solution.py:173
  118.1 2.8 %fusion.8 = f32[16,1,16,192]{3,2,0,1:T(8,128)S(1)} fusion(bf16[16,16,4096]{2,1,0:T(8,128)(2,1)} %get-tuple-element.14, bf16[1,4096,192]{1,2,0:T(8,128)(2,1)} %param.37), kind=kOutput, calls=%fused_computation.15 | convolution fusion | flops 402653184 | bytes 3866624 | tf_op jit(solution)/shard_map/sxcd,xdf->sxcf/dot_general | solution.py:541
  120.9 5.9 %convolution_convert_fusion.refs_2_ = bf16[16,16,4096]{2,1,0:T(8,128)(2,1)} fusion(bf16[1,192,4096]{2,1,0:T(8,128)(2,1)S(1)} %copy-done, bf16[16,16,4096]{2,1,0:T(8,128)(2,1)} %get-tuple-element.14, bf16[1,4096,192]{1,2,0:T(8,128)(2,1)} %param.38, f32[16,1,16,192]{3,2,0,1:T(8,128)S(1)} %fusion.8), kind=kOutput, calls=%fused_computation | convolution fusion | flops 806649856 | bytes 7536640 | tf_op jit(solution)/shard_map/sxcf,xfd->sxcd/dot_general | solution.py:546
  126.7 2.5 %fusion.64 = f32[256,128]{1,0:T(8,128)S(1)} fusion(bf16[256,4096]{1,0:T(8,128)(2,1)} %get-tuple-element.13, bf16[4096,128]{1,0:T(8,128)(2,1)S(1)} %copy-done.4), kind=kOutput, calls=%fused_computation.88 | convolution fusion | flops 268435456 | bytes 3276800 | tf_op jit(solution)/shard_map/dot_general | solution.py:549
  129.2 1.3 fusion.26.refs_0_
  130.6 54.0 %shard_map.203 = (f32[64,4096]{1,0:T(8,128)}, bf16[16,16,4096]{2,1,0:T(8,128)(2,1)}) custom-call(bf16[256,128]{1,0:T(8,128)(2,1)} %fusion.26.refs_0_, bf16[128,4096]{1,0:T(8,128)(2,1)} %refs_1_.1, bf16[16,16,4096]{2,1,0:T(8,128)(2,1)} %convolution_convert_fusion.refs_2_), custom_call_target="tpu_custom_call" | custom-call | bytes 40000000 | tf_op jit(solution)/shard_map/pallas_call | solution.py:272
  184.6 2.3 %convolution_multiply_fusion.1 = f32[64,4096]{1,0:T(8,128)S(1)} fusion(bf16[256,4096]{1,0:T(8,128)(2,1)} %bitcast.83, f32[64]{0:T(128)S(1)} %get-tuple-element.24, s32[64]{0:T(128)S(1)} %get-tuple-element.22), kind=kOutput, calls=%fused_computation.4 | convolution fusion | flops 134496256 | bytes 3146240 | tf_op jit(solution)/shard_map/dot_general | solution.py:560
  186.9 0.2 copy-done.5
  187.0 1.5 fusion.2
  (34 shorter events, 0.4 us)
Async XLA Ops:
  0.0 120.9 %copy-start = (bf16[1,192,4096]{2,1,0:T(8,128)(2,1)S(1)}, bf16[1,192,4096]{2,1,0:T(8,128)(2,1)}, u32[]{:S(2)}) copy-start(bf16[1,192,4096]{2,1,0:T(8,128)(2,1)} %param.39) | copy-start | bytes 4718596
  32.9 19.3 %copy-start.6 = (bf16[64,4096]{1,0:T(8,128)(2,1)S(1)}, bf16[64,4096]{1,0:T(8,128)(2,1)}, u32[]{:S(2)}) copy-start(bf16[64,4096]{1,0:T(8,128)(2,1)} %param.32) | copy-start | bytes 1572868
  52.2 1.5 copy-start.7
  52.3 1.7 copy-start.8
  54.0 2.9 %copy-start.2 = (bf16[64,4096]{1,0:T(8,128)(2,1)}, bf16[64,4096]{1,0:T(8,128)(2,1)S(1)}, u32[]{:S(2)}) copy-start(bf16[64,4096]{1,0:T(8,128)(2,1)S(1)} %fusion.33.refs_0_) | copy-start | bytes 1572868
  120.9 5.9 %copy-start.4 = (bf16[4096,128]{1,0:T(8,128)(2,1)S(1)}, bf16[4096,128]{1,0:T(8,128)(2,1)}, u32[]{:S(2)}) copy-start(bf16[4096,128]{1,0:T(8,128)(2,1)} %param.34) | copy-start | bytes 3145732
  126.7 2.5 %copy-start.3 = (bf16[256,4096]{1,0:T(8,128)(2,1)S(1)}, bf16[256,4096]{1,0:T(8,128)(2,1)}, u32[]{:S(2)}) copy-start(bf16[256,4096]{1,0:T(8,128)(2,1)} %get-tuple-element.13) | copy-start | bytes 6291460
  126.7 2.5 %copy-start.10 = (bf16[4096,128]{1,0:T(8,128)(2,1)S(1)}, bf16[4096,128]{1,0:T(8,128)(2,1)}, u32[]{:S(2)}) copy-start(bf16[4096,128]{1,0:T(8,128)(2,1)} %param.35) | copy-start | bytes 3145732
  130.6 54.0 %copy-start.9 = (f32[64,2]{0,1:T(2,128)S(1)}, f32[64,2]{0,1:T(2,128)}, u32[]{:S(2)}) copy-start(f32[64,2]{0,1:T(2,128)} %param.41) | copy-start | bytes 1540
  184.5 2.3 %copy-start.1 = (bf16[16,16,4096]{2,1,0:T(8,128)(2,1)S(1)}, bf16[16,16,4096]{2,1,0:T(8,128)(2,1)}, u32[]{:S(2)}) copy-start(bf16[16,16,4096]{2,1,0:T(8,128)(2,1)} %get-tuple-element.16) | copy-start | bytes 6291460
  184.5 2.5 %copy-start.5 = (f32[64,4096]{1,0:T(8,128)S(1)}, f32[64,4096]{1,0:T(8,128)}, u32[]{:S(2)}) copy-start(f32[64,4096]{1,0:T(8,128)} %get-tuple-element.15) | copy-start | bytes 3145732
where the time goes:
time: 189 us; the launch traced here: 188 us
  Pallas kernels  160 us (85%)
  matrix products  21.1 us (11%)
  other arithmetic  5.99 us (3%)
    pallas_call x2, Pallas kernels, dot_scatter(): pl.pallas_call(lambda *refs: scatter_kernel(n_tp, pieces, pairs, moving,...  73.3 us
    pallas_call x1, Pallas kernels, gather_rows(): pl.pallas_call(lambda *refs: gather_kernel(n_tp, pieces, *refs), out_shap...  61.2 us
    pallas_call x1, Pallas kernels, spread(): pl.pallas_call(lambda *refs: spread_kernel(n_sp, n_tp, *refs), out_shape=...  20.1 us
    pallas_call x1, Pallas kernels, attend(): pl.pallas_call(lambda *refs: attend_kernel(sizes, *refs), out_shape=[jax....  5.87 us
    dot_general x1, matrix products, body(): jnp.einsum('sxcf,xfd->sxcd', active, expert_down, preferred_element_type=...  5.86 us

commit v1 on v0

--- a/solution.py
+++ b/solution.py
@@ -53,12 +53,22 @@
     )
 
 
-def spread_kernel(n_sp, n_tp, x_ref, out_ref, z_send, z_recv, t_send, t_recv, own_sem):
+def spread_kernel(n_sp, n_tp, x_ref, *refs):
+    if len(refs) > 6:
+        meta_ref, out_ref, all_ref = refs[:3]
+        z_send, z_recv, t_send, t_recv, own_sem = refs[3:8]
+        toll = Exchange(None, None, *refs[8:11])
+    else:
+        out_ref, z_send, z_recv, t_send, t_recv, own_sem = refs
+        toll = None
     sp, tp = lax.axis_index("sp"), lax.axis_index("tp")
     tok = x_ref.shape[0]
     part = tok // n_tp
     targets = [{"sp": lax.rem(sp + r, n_sp)} for r in range(1, n_sp)]
-    greet(targets + [{"tp": flip(tp, m)} for m in masks_of(n_tp)])
+    if toll is None:
+        greet(targets + [{"tp": flip(tp, m)} for m in masks_of(n_tp)])
+    else:
+        toll.greet()
 
     def rows(block, member):
         return pl.ds(pl.multiple_of(block * tok + member * part, part), part)
@@ -78,6 +88,11 @@
         copy.start()
         sends.append(copy)
     own.start()
+    if toll is not None:
+        tolls = [toll.toll(k, meta_ref, all_ref) for k in range(1, toll.count)]
+        for copy in tolls:
+            copy.start()
+        all_ref[toll.me] = meta_ref[...]
 
     def piece(r, d):
         return out_ref.at[rows(lax.rem(sp + n_sp - r, n_sp), flip(tp, d))]
@@ -104,25 +119,35 @@
     for copy in sends:
         copy.wait_send()
     own.wait()
-
-
-def spread(x, n_sp, n_tp):
+    if toll is not None:
+        for copy in tolls:
+            copy.wait()
+
+
+def spread(x, n_sp, n_tp, meta=None):
     tok, width = x.shape
+    out_shape = [jax.ShapeDtypeStruct((n_sp * tok, width), x.dtype)]
+    operands, extra = (x,), []
+    if meta is not None:
+        operands += (meta,)
+        out_shape.append(jax.ShapeDtypeStruct((n_sp * n_tp,) + meta.shape, meta.dtype))
+        extra = exchange_semaphores(n_sp * n_tp)
     return pl.pallas_call(
         lambda *refs: spread_kernel(n_sp, n_tp, *refs),
-        out_shape=jax.ShapeDtypeStruct((n_sp * tok, width), x.dtype),
-        in_specs=[VMEM],
-        out_specs=VMEM,
+        out_shape=out_shape,
+        in_specs=[VMEM] * len(operands),
+        out_specs=[VMEM] * len(out_shape),
         scratch_shapes=[
             pltpu.SemaphoreType.DMA((n_sp,)),
             pltpu.SemaphoreType.DMA((n_sp,)),
             pltpu.SemaphoreType.DMA((n_sp, n_tp)),
             pltpu.SemaphoreType.DMA((n_sp, n_tp)),
             pltpu.SemaphoreType.DMA,
-        ],
+        ]
+        + extra,
         compiler_params=pltpu.CompilerParams(collective_id=0, has_side_effects=True),
         cost_estimate=pl.CostEstimate(flops=0, bytes_accessed=30_000_000, transcendentals=0),
-    )(x)
+    )(*operands)
 
 
 def gather_kernel(
@@ -278,6 +303,422 @@
         compiler_params=pltpu.CompilerParams(collective_id=collective, has_side_effects=True),
         cost_estimate=pl.CostEstimate(flops=0, bytes_accessed=40_000_000, transcendentals=0),
     )(*operands)
+
+
+def moe_kernel(chunks, cap, *refs):
+    x_ref, stream_ref, meta_ref = refs[:3]
+    hbm = refs[3:9]
+    out_ref = refs[9]
+    blk, plane, gbuf, crow, obuf, ret, chs, chin, fin, sent, got = refs[10:21]
+    local = refs[21:27]
+    sg, su, sd, eg, eu, ed = local
+    smat, som, wcol, hg, hu, act, shg, shu, sact, facc = refs[27:37]
+    wsem, psend, precv, csend, crecv, gsend, grecv, osend, orecv = refs[37:46]
+    dsend, drecv, frecv, rsend, rrecv = refs[46:51]
+    z, tp = lax.axis_index("sp"), lax.axis_index("tp")
+    n_sp, n_tp = lax.axis_size("sp"), lax.axis_size("tp")
+    rows, width = x_ref.shape
+    part = width // chunks
+    slots = n_tp * cap
+    way = 1 - 2 * (z // 2)
+    f32, bf16 = jnp.float32, jnp.bfloat16
+
+    def cols(q):
+        return pl.ds(pl.multiple_of(q * part, part), part)
+
+    def peer(d):
+        return {"tp": flip(tp, d)}
+
+    def dot(a, b):
+        return jnp.dot(a, b, preferred_element_type=f32)
+
+    def dot_nt(a, b):
+        return lax.dot_general(a, b, (((1,), (1,)), ((), ())), preferred_element_type=f32)
+
+    def dot_tn(a, b):
+        return lax.dot_general(a, b, (((0,), (0,)), ((), ())), preferred_element_type=f32)
+
+    barrier = pltpu.get_barrier_semaphore()
+
+    def signal(target):
+        pl.semaphore_signal(barrier, inc=1, device_id=target, device_id_type=MESH)
+
+    for d in range(1, n_tp):
+        signal(peer(d))
+
+    @pl.when(z > 0)
+    def _():
+        signal({"sp": z - 1})
+
+    @pl.when(z < n_sp - 1)
+    def _():
+        signal({"sp": z + 1})
+
+    loads = [
+        pltpu.make_async_copy(a, b, wsem.at[k]) for k, (a, b) in enumerate(zip(hbm, local))
+    ]
+    for k in (3, 4, 0, 1, 5, 2):
+        loads[k].start()
+    pl.semaphore_wait(
+        barrier, n_tp - 1 + (z + n_sp - 1) // n_sp + (2 * n_sp - 2 - z) // n_sp
+    )
+
+    def block_out(p, q, k, target, source=None):
+        source = blk.at[p, :, cols(q)] if source is None else source
+        return remote(source, blk.at[p, :, cols(q)], csend.at[k, q], crecv.at[p, q], target)
+
+    def own_out(q, step):
+        return block_out(z, q, (1 - step) // 2, {"sp": z + step}, x_ref.at[:, cols(q)])
+
+    def gather_out(m, q):
+        return remote(
+            x_ref.at[:, cols(q)],
+            plane.at[pl.ds(m * rows, rows), cols(q)],
+            psend.at[m, q],
+            precv.at[m, q],
+            peer(m),
+        )
+
+    def gather_on(q):
+        return remote(
+            plane.at[pl.ds(2 * rows, rows), cols(q)],
+            plane.at[pl.ds(3 * rows, rows), cols(q)],
+            psend.at[3, q],
+            precv.at[3, q],
+            peer(1),
+        )
+
+    for q in range(chunks):
+
+        @pl.when(z < n_sp - 1)
+        def _():
+            own_out(q, 1).start()
+
+        @pl.when(z > 0)
+        def _():
+            own_out(q, -1).start()
+
+        if q == 0:
+            gather_out(2, 0).start()
+            gather_out(1, 0).start()
+
+    plane[:rows, :] = x_ref[...]
+    hg[...] = jnp.zeros_like(hg)
+    hu[...] = jnp.zeros_like(hu)
+    shg[...] = jnp.zeros_like(shg)
+    shu[...] = jnp.zeros_like(shu)
+    som[...] = jnp.zeros_like(som)
+    lanes = meta_ref.shape[2]
+    iota = lax.broadcasted_iota(jnp.int32, (cap, lanes), 0)
+    for step in range(n_sp):
+        p = lax.rem(z + step, n_sp)
+        for d in range(n_tp):
+            if step:
+                info = meta_ref[p * n_tp + tp]
+                slot = ((z * n_tp + flip(tp, d)) * cap + iota).astype(f32)
+                hit = (info[0:1, :] == slot) | (info[1:2, :] == slot)
+                smat[p, d * cap : (d + 1) * cap, :] = hit.astype(f32)[:, :rows].astype(bf16)
+            info = meta_ref[p * n_tp + flip(tp, d)]
+            slot = ((z * n_tp + tp) * cap + iota).astype(f32)
+            first, second = info[0:1, :] == slot, info[1:2, :] == slot
+            weight = jnp.where(first, info[2:3, :], 0.0) + jnp.where(second, info[3:4, :], 0.0)
+            wcol[p, d * cap : (d + 1) * cap, :] = jnp.sum(weight, axis=1, keepdims=True)
+            if not step:
+                hit = (first | second).astype(f32)[:, :rows].astype(bf16)
+                som[d * cap : (d + 1) * cap, d * rows : (d + 1) * rows] = hit
+
+    def piece(p, d, q):
+        return p, pl.ds(d * cap, cap), cols(q)
+
+    def spread_out(p, d, q):
+        at = piece(p, d, q)
+        return remote(gbuf.at[at], crow.at[at], gsend.at[p, d, q], grecv.at[p, d, q], peer(d))
+
+    def c_unit(p, q, k=None, target=None):
+        block_out(p, q, 0, peer(1)).wait_recv()
+        if k is not None:
+            block_out(p, q, k, target).start()
+        picked = dot(smat[p], blk[p, :, cols(q)]).astype(bf16)
+        gbuf[p, :, cols(q)] = picked
+        crow[p, :cap, cols(q)] = picked[:cap]
+        for d in (2, 3, 1):
+            spread_out(p, d, q).start()
+
+    def hidden(p, q):
+        taken = crow[p, :, cols(q)]
+        hg[p] += dot_nt(taken, eg[:, cols(q)])
+        hu[p] += dot_nt(taken, eu[:, cols(q)])
+
+    def h_unit(p, q):
+        for d in (1, 2, 3):
+            spread_out(p, d, q).wait_recv()
+        hidden(p, q)
+
+    def activate(p):
+        gate = hg[p]
+        act[p] = (gate / (1.0 + jnp.exp(-gate)) * hu[p]).astype(bf16)
+
+    def own_unit(q):
+        @pl.when(q < chunks - 1)
+        def _():
+            gather_out(2, q + 1).start()
+            gather_out(1, q + 1).start()
+
+        gather_out(2, q).wait_recv()
+        gather_on(q).start()
+        gather_out(1, q).wait_recv()
+        gather_on(q).wait_recv()
+        full = plane[:, cols(q)]
+        crow[z, :, cols(q)] = dot(som[...], full).astype(bf16)
+        deep = pl.ds(pl.multiple_of(q * part, part), part)
+        shg[...] += dot(full, sg[deep, :])
+        shu[...] += dot(full, su[deep, :])
+        hidden(z, q)
+
+    def own_activate():
+        activate(z)
+        gate = shg[...]
+        sact[...] = (gate / (1.0 + jnp.exp(-gate)) * shu[...]).astype(bf16)
+
+    def outcome(p, q):
+        made = dot(act[p], ed[:, cols(q)]).astype(bf16).astype(f32)
+        return (made * wcol[p]).astype(bf16)
+
+    def back_out(p, d, q):
+        at = piece(p, d, q)
+        return remote(obuf.at[at], ret.at[at], osend.at[p, d, q], orecv.at[p, d, q], peer(d))
+
+    def o_unit(p, q):
+        made = outcome(p, q)
+        obuf[p, :, cols(q)] = made
+        ret[p, :cap, cols(q)] = made[:cap]
+        for d in (2, 3, 1):
+            back_out(p, d, q).start()
+
+    def chain_out(p, q, last, step):
+        into, sem = chin.at[p, :, cols(q)], drecv.at[p, q]
+        if last:
+            side = (1 - step) // 2
+            into, sem = fin.at[side, :, cols(q)], frecv.at[side, q]
+        return remote(chs.at[p, :, cols(q)], into, dsend.at[p, q], sem, {"sp": z + step})
+
+    def d_unit(p, q, incoming, last, step):
+        for d in (1, 2, 3):
+            back_out(p, d, q).wait_recv()
+        total = dot_tn(smat[p], ret[p, :, cols(q)])
+        if incoming:
+            chain_out(p, q, False, step).wait_recv()
+            total = total + chin[p, :, cols(q)].astype(f32)
+        chs[p, :, cols(q)] = total.astype(bf16)
+        chain_out(p, q, last, step).start()
+
+    def product(d, q):
+        return dot(sact[d * rows : (d + 1) * rows, :], sd[:, cols(q)]) + dot_tn(
+            som[:, d * rows : (d + 1) * rows], obuf[z, :, cols(q)]
+        )
+
+    def fold(d, q, mask):
+        return remote(
+            sent.at[d, :, cols(q)],
+            got.at[d, :, cols(q)],
+            rsend.at[d, q],
+            rrecv.at[d, q],
+            peer(mask),
+        )
+
+    def rs1(q):
+        obuf[z, :, cols(q)] = outcome(z, q)
+        for d in (3, 1):
+            sent[d, :, cols(q)] = product(d, q).astype(bf16)
+            fold(d, q, 1).start()
+
+    def rs2(q):
+        total = product(2, q)
+        fold(3, q, 1).wait_recv()
+        sent[2, :, cols(q)] = (total + got[3, :, cols(q)].astype(f32)).astype(bf16)
+        fold(2, q, 2).start()
+
+    def base(q):
+        total = product(0, q) + stream_ref[:, cols(q)].astype(f32)
+        fold(1, q, 1).wait_recv()
+        total = total + got[1, :, cols(q)].astype(f32)
+        fold(2, q, 2).wait_recv()
+        facc[:, cols(q)] = total + got[2, :, cols(q)].astype(f32)
+
+    def arrive(side, q):
+        remote(
+            fin.at[side, :, cols(q)],
+            fin.at[side, :, cols(q)],
+            dsend.at[0, q],
+            frecv.at[side, q],
+            peer(1),
+        ).wait_recv()
+        return fin[side, :, cols(q)].astype(f32)
+
+    def staged(first, later=None):
+        def one(q, carry):
+            @pl.when(q < chunks)
+            def _():
+                first(q)
+
+            if later is not None:
+
+                @pl.when(q > 0)
+                def _():
+                    later(q - 1)
+
+            return carry
+
+        lax.fori_loop(0, chunks + (later is not None), one, 0)
+
+    def run(*steps):
+        def each(q):
+            for step in steps:
+                step(q)
+
+        return each
+
+    def sends_done(copies):
+        def one(q, carry):
+            for copy in copies(q):
+                copy.wait_send()
+            return carry
+
+        lax.fori_loop(0, chunks, one, 0)
+
+    for k in (3, 4, 0, 1, 5, 2):
+        loads[k].wait()
+
+    is_end = (z == 0) | (z == n_sp - 1)
+
+    @pl.when(is_end)
+    def _():
+        p0, p1, p2 = z + way, z + 2 * way, z + 3 * way
+        staged(run(own_unit, lambda q: c_unit(p0, q)), lambda q: h_unit(p0, q))
+        activate(p0)
+        own_activate()
+        staged(
+            run(lambda q: c_unit(p1, q), lambda q: o_unit(p0, q)),
+            run(lambda q: h_unit(p1, q), lambda q: d_unit(p0, q, False, True, way)),
+        )
+        activate(p1)
+        staged(
+            run(lambda q: c_unit(p2, q), lambda q: o_unit(p1, q), rs1),
+            run(lambda q: h_unit(p2, q), lambda q: d_unit(p1, q, False, False, way)),
+        )
+        activate(p2)
+        staged(
+            run(lambda q: o_unit(p2, q), rs2), lambda q: d_unit(p2, q, False, False, way)
+        )
+        staged(base)
+
+        def last(q):
+            out_ref[:, cols(q)] = (facc[:, cols(q)] + arrive((1 + way) // 2, q)).astype(bf16)
+
+        staged(last)
+        sends_done(
+            lambda q: [own_out(q, way)]
+            + [spread_out(p, d, q) for p in (p0, p1, p2) for d in (1, 2, 3)]
+            + [back_out(p, d, q) for p in (p0, p1, p2) for d in (1, 2, 3)]
+            + [chain_out(p, q, False, way) for p in (p0, p1, p2)]
+        )
+
+    @pl.when(jnp.logical_not(is_end))
+    def _():
+        s0, s1, s2 = z - way, z + way, z + 2 * way
+        ahead, behind = {"sp": z + way}, {"sp": z - way}
+        staged(
+            run(
+                lambda q: c_unit(s0, q, 2, ahead),
+                lambda q: c_unit(s1, q, 3, behind),
+                own_unit,
+            ),
+            run(lambda q: h_unit(s0, q), lambda q: h_unit(s1, q)),
+        )
+        activate(s0)
+        activate(s1)
+        own_activate()
+        staged(
+            run(lambda q: c_unit(s2, q, 4, behind), lambda q: o_unit(s1, q), rs1),
+            run(lambda q: h_unit(s2, q), rs2),
+        )
+        activate(s2)
+        staged(
+            run(lambda q: o_unit(s2, q), lambda q: o_unit(s0, q)),
+            run(lambda q: d_unit(s1, q, True, True, way), base),
+        )
+        staged(
+            run(
+                lambda q: d_unit(s2, q, True, False, way),
+                lambda q: d_unit(s0, q, True, True, -way),
+            )
+        )
+
+        def last(q):
+            total = facc[:, cols(q)] + arrive(0, q) + arrive(1, q)
+            out_ref[:, cols(q)] = total.astype(bf16)
+
+        staged(last)
+        sends_done(
+            lambda q: [own_out(q, way), own_out(q, -way)]
+            + [block_out(s0, q, 2, ahead), block_out(s1, q, 3, behind)]
+            + [block_out(s2, q, 4, behind)]
+            + [spread_out(p, d, q) for p in (s0, s1, s2) for d in (1, 2, 3)]
+            + [back_out(p, d, q) for p in (s0, s1, s2) for d in (1, 2, 3)]
+            + [chain_out(p, q, False, way) for p in (s0, s1, s2)]
+        )
+
+    sends_done(
+        lambda q: [gather_out(2, q), gather_out(1, q), gather_on(q)]
+        + [fold(3, q, 1), fold(1, q, 1), fold(2, q, 2)]
+    )
+
+
+def moe(normed, stream, meta, weights, n_sp, n_tp, cap, chunks=4):
+    rows, width = normed.shape
+    sg, su, sd, eg, eu, ed = weights
+    slots = n_tp * cap
+    hidden, share = eg.shape[0], sg.shape[1]
+    bf16, f32 = jnp.bfloat16, jnp.float32
+    any_space = pl.BlockSpec(memory_space=pl.ANY)
+    per_plane = pltpu.VMEM((n_sp, slots, width), bf16)
+    blocks = pltpu.VMEM((n_sp, rows, width), bf16)
+    folds = pltpu.VMEM((n_tp, rows, width), bf16)
+
+    def sems(*shape):
+        return pltpu.SemaphoreType.DMA(shape)
+
+    scratch = [blocks, pltpu.VMEM((n_tp * rows, width), bf16)]
+    scratch += [per_plane] * 4 + [blocks] * 2
+    scratch += [pltpu.VMEM((2, rows, width), bf16), folds, folds]
+    scratch += [pltpu.VMEM(w.shape, w.dtype) for w in weights]
+    scratch += [
+        pltpu.VMEM((n_sp, slots, rows), bf16),
+        pltpu.VMEM((slots, n_tp * rows), bf16),
+        pltpu.VMEM((n_sp, slots, 1), f32),
+        pltpu.VMEM((n_sp, slots, hidden), f32),
+        pltpu.VMEM((n_sp, slots, hidden), f32),
+        pltpu.VMEM((n_sp, slots, hidden), bf16),
+        pltpu.VMEM((n_tp * rows, share), f32),
+        pltpu.VMEM((n_tp * rows, share), f32),
+        pltpu.VMEM((n_tp * rows, share), bf16),
+        pltpu.VMEM((rows, width), f32),
+    ]
+    scratch += [sems(6), sems(n_tp, chunks), sems(n_tp, chunks)]
+    scratch += [sems(5, chunks), sems(n_sp, chunks)]
+    scratch += [sems(n_sp, n_tp, chunks)] * 4
+    scratch += [sems(n_sp, chunks), sems(n_sp, chunks), sems(2, chunks)]
+    scratch += [sems(n_tp, chunks), sems(n_tp, chunks)]
+    return pl.pallas_call(
+        lambda *refs: moe_kernel(chunks, cap, *refs),
+        out_shape=jax.ShapeDtypeStruct((rows, width), bf16),
+        in_specs=[VMEM] * 3 + [any_space] * 6,
+        out_specs=VMEM,
+        scratch_shapes=scratch,
+        compiler_params=pltpu.CompilerParams(
+            collective_id=4, has_side_effects=True, vmem_limit_bytes=60 << 20
+        ),
+    )(normed, stream, meta, *weights)
 
 
 EPS = 1e-06
@@ -396,7 +837,13 @@
         self.n_sp, self.n_tp = lax.axis_size("sp"), lax.axis_size("tp")
         self.count = self.n_sp * self.n_tp
         self.me = self.sp * self.n_tp + self.tp
-        self.own = pltpu.make_async_copy(source.at[self.me], dest.at[self.me], own_sem)
+        if source is not None:
+            self.own = pltpu.make_async_copy(source.at[self.me], dest.at[self.me], own_sem)
+
+    def toll(self, k, source, dest):
+        sp, tp = self.target(k)
+        send, recv = self.refs[2:]
+        return remote(source, dest.at[self.me], send.at[k], recv.at[k], {"sp": sp, "tp": tp})
 
     def target(self, k):
         return (
@@ -499,7 +946,30 @@
         jnp.dot(rope_key, same, preferred_element_type=jnp.float32) * cosine
         + jnp.dot(rope_key, cross.astype(jnp.bfloat16), preferred_element_type=jnp.float32) * sine
     ).astype(jnp.bfloat16)
-    packed = spread(jnp.concatenate([normed_latent, turned_key], axis=1), n_sp, n_tp)
+    rows_here, top_count = routes.shape
+    local_experts = expert_gate.shape[0]
+    experts_all = local_experts * lax.axis_size(("sp", "tp"))
+    capacity = max(2, 2 * top_count * rows_here // experts_all)
+    flat_routes = routes.reshape(-1)
+    assigned = flat_routes.shape[0]
+    choose = (flat_routes[:, None] == jnp.arange(experts_all, dtype=jnp.int32)[None, :]).astype(
+        jnp.float32
+    )
+    lower_mask = (jnp.arange(assigned)[:, None] > jnp.arange(assigned)[None, :]).astype(jnp.float32)
+    earlier = jnp.dot(lower_mask, choose, precision=lax.Precision.HIGHEST)
+    slots = jnp.sum(earlier * choose, axis=1).astype(jnp.int32)
+    target = flat_routes * capacity + slots
+    by_choice = target.reshape(rows_here, top_count)
+    planes = n_sp == 4 and n_tp == 4 and local_experts == 1 and capacity % 16 == 0
+    fused = planes and top_count == 2 and rows_here <= 128
+    rows_packed = jnp.concatenate([normed_latent, turned_key], axis=1)
+    if fused:
+        spare = (-rows_here) % 128
+        facts = jnp.concatenate([by_choice.astype(jnp.float32).T, route_weights.T], axis=0)
+        facts = jnp.pad(facts, ((0, 4), (0, spare)), constant_values=-1.0)
+        packed, meta = spread(rows_packed, n_sp, n_tp, facts)
+    else:
+        (packed,) = spread(rows_packed, n_sp, n_tp)
     wide_mix, narrow_mix = attend(
         packed,
         cosine,
@@ -512,20 +982,11 @@
     (projected,) = dot_scatter((wide_mix, narrow_mix), (out_wide, out_narrow), n_tp, 2)
     stream = (residual.astype(jnp.float32) + projected).astype(jnp.bfloat16)
     normed = rms_scale(stream.astype(jnp.float32), ffn_gain).astype(jnp.bfloat16)
-    rows_here, top_count = routes.shape
-    local_experts = expert_gate.shape[0]
-    experts_all = local_experts * lax.axis_size(("sp", "tp"))
-    capacity = max(2, 2 * top_count * rows_here // experts_all)
+    if fused:
+        weights = (shared_gate, shared_up, shared_down)
+        weights += (expert_gate[0].T, expert_up[0].T, expert_down[0])
+        return moe(normed, stream, meta, weights, n_sp, n_tp, capacity)
     model_width = normed.shape[1]
-    flat_routes = routes.reshape(-1)
-    assigned = flat_routes.shape[0]
-    choose = (flat_routes[:, None] == jnp.arange(experts_all, dtype=jnp.int32)[None, :]).astype(
-        jnp.float32
-    )
-    lower_mask = (jnp.arange(assigned)[:, None] > jnp.arange(assigned)[None, :]).astype(jnp.float32)
-    earlier = jnp.dot(lower_mask, choose, precision=lax.Precision.HIGHEST)
-    slots = jnp.sum(earlier * choose, axis=1).astype(jnp.int32)
-    target = flat_routes * capacity + slots
     send_map = jnp.any(
         target.reshape(rows_here, top_count)[None, :, :]
         == jnp.arange(experts_all * capacity, dtype=jnp.int32)[:, None, None],
@@ -553,7 +1014,6 @@
         (active,), (shared_down,), n_tp, 3, finished.reshape(outgoing.shape)
     )
     slot_rows = returned.reshape(experts_all * capacity, model_width)
-    by_choice = target.reshape(rows_here, top_count)
     routed = jnp.zeros((rows_here, model_width), jnp.float32)
     for choice in range(top_count):
         hot = by_choice[:, choice : choice + 1] == jnp.arange(experts_all * capacity)[None, :]

time: 189 us -> 156 us (0.83)
  matrix products: 21.1 us -> 1.21 us
  Pallas kernels: 160 us -> 144 us
  local copies, waits for them, and re-layouts: 0.67 us -> 3.05 us
    pallas_call x2 -> x1, Pallas kernels: 73.3 us -> 19.3 us  [dot_scatter(): pl.pallas_call(lambda *refs: scatter_kernel(n_tp, pieces, pairs, moving,...]
    pallas_call x1, Pallas kernels: 61.2 us -> 96.8 us  [moe(): pl.pallas_call(lambda *refs: moe_kernel(chunks, cap, *refs), out_shape=ja...]
    dot_general x7 -> x0, matrix products: 18.2 us -> none  [the longest x1 5.86 us: body(): jnp.einsum('sxcf,xfd->sxcd', active, expert_down, preferred_element_type=...]
    unnamed x23 -> x14, local copies, waits for them, and re-layouts: 0.31 us -> 2.7 us
where the time goes in v1:
time: 156 us; the launch traced here: 155 us
  Pallas kernels  144 us (92%)
  other arithmetic  7.27 us (5%)
  local copies, waits for them, and re-layouts  3.05 us (2%)
    pallas_call x1, Pallas kernels, moe(): pl.pallas_call(lambda *refs: moe_kernel(chunks, cap, *refs), out_shape=ja...  96.8 us
    pallas_call x1, Pallas kernels, spread(): pl.pallas_call(lambda *refs: spread_kernel(n_sp, n_tp, *refs), out_shape=...  22 us
    pallas_call x1, Pallas kernels, dot_scatter(): pl.pallas_call(lambda *refs: scatter_kernel(n_tp, pieces, pairs, moving,...  19.3 us
    pallas_call x1, Pallas kernels, attend(): pl.pallas_call(lambda *refs: attend_kernel(sizes, *refs), out_shape=[jax....  5.69 us

profile of v1, /device:TPU:0, one launch (start us, length us, event | category | flops | bytes accessed | tf_op | source)
XLA Modules:
  0.0 155.5 jit_solution(12459746391146239943)
XLA Ops:
  0.0 0.0 copy-start
  0.1 0.7 copy-done
  0.8 0.5 fusion.2
  1.3 0.5 fusion.3
  1.8 1.1 fusion.8
  2.9 1.1 fusion.10
  4.0 0.8 pad_maximum_fusion.refs_0_
  4.8 0.0 copy-done.4
  4.8 0.1 copy.28
  4.9 0.1 eq.62
  5.0 0.2 fusion.4
  5.2 0.1 convert_element_type.69
  5.3 0.1 copy.29
  5.4 0.6 select_maximum_fusion.refs_1_
  6.0 22.0 %shard_map.199 = (bf16[1024,640]{1,0:T(8,128)(2,1)}, f32[16,8,128]{2,1,0:T(8,128)}) custom-call(bf16[256,640]{1,0:T(8,128)(2,1)} %pad_maximum_fusion.refs_0_, f32[8,128]{1,0:T(8,128)} %select_maximum_fusion.refs_1_), custom_call_target="tpu_custom_call" | custom-call | bytes 30000000 | tf_op jit(solution)/shard_map/pallas_call | solution.py:135
  28.0 1.2 multiply_sine_fusion
  29.2 5.7 %shard_map.200 = (bf16[256,256]{1,0:T(8,128)(2,1)}, bf16[256,128]{1,0:T(8,128)(2,1)}) custom-call(bf16[1024,640]{1,0:T(8,128)(2,1)} %get-tuple-element.9.refs_0_, f32[256,128]{1,0:T(8,128)} %get-tuple-element.16.refs_1_, f32[256,128]{1,0:T(8,128)} %get-tuple-element.15.refs_2_, bf16[256,384]{1,0:T(8,128)(2,1)} %refs_3_.3, bf16[256,256]{1,0:T(8,128)(2,1)} %refs_4_.2, ...), custom_call_target="tpu_custom_call" | custom-call | tf_op jit(solution)/shard_map/pallas_call | solution.py:824
  34.9 19.3 %shard_map.201 = f32[64,4096]{1,0:T(8,128)} custom-call(bf16[256,256]{1,0:T(8,128)(2,1)} %get-tuple-element.10.refs_0_, bf16[256,128]{1,0:T(8,128)(2,1)} %get-tuple-element.11.refs_1_, bf16[256,4096]{1,0:T(8,128)(2,1)} %refs_2_.1, bf16[128,4096]{1,0:T(8,128)(2,1)} %refs_3_.4), custom_call_target="tpu_custom_call" | custom-call | bytes 40000000 | tf_op jit(solution)/shard_map/pallas_call | solution.py:297
  54.3 0.0 copy-start.3
  54.3 1.5 fusion.5
  55.8 0.0 copy-done.3
  55.8 1.0 fusion.7.refs_0_
  56.8 96.8 %shard_map.202 = bf16[64,4096]{1,0:T(8,128)(2,1)} custom-call(bf16[64,4096]{1,0:T(8,128)(2,1)} %fusion.7.refs_0_, bf16[64,4096]{1,0:T(8,128)(2,1)} %copy-done.1, f32[16,8,128]{2,1,0:T(8,128)} %get-tuple-element.12.refs_2_, bf16[4096,128]{1,0:T(8,128)(2,1)} %refs_3_.5, bf16[4096,128]{1,0:T(8,128)(2,1)} %refs_4_.3, bf16[128,4096]{1,0:T(8,128)(2,1)} %refs_5_.3, ...), custom_call_target="tpu_custom_call" | custom-call | tf_op jit(solution)/shard_map/pallas_call | solution.py:712
  153.6 1.9 %copy.33 = bf16[64,4096]{1,0:T(8,128)(2,1)} copy(bf16[64,4096]{1,0:T(8,128)(2,1)} %shard_map.202) | data formatting | bytes 1048576
  (15 shorter events, 0.1 us)
Async XLA Ops:
  0.0 0.8 copy-start
  0.0 4.8 %copy-start.4 = (s32[64,2]{0,1:T(2,128)S(1)}, s32[64,2]{0,1:T(2,128)}, u32[]{:S(2)}) copy-start(s32[64,2]{0,1:T(2,128)} %param.40) | copy-start | bytes 1540
  0.0 5.4 %copy-start.5 = (f32[64,2]{0,1:T(2,128)S(1)}, f32[64,2]{0,1:T(2,128)}, u32[]{:S(2)}) copy-start(f32[64,2]{0,1:T(2,128)} %param.41) | copy-start | bytes 1540
  34.9 19.3 %copy-start.2 = (bf16[64,4096]{1,0:T(8,128)(2,1)S(1)}, bf16[64,4096]{1,0:T(8,128)(2,1)}, u32[]{:S(2)}) copy-start(bf16[64,4096]{1,0:T(8,128)(2,1)} %param.32) | copy-start | bytes 1572868
  54.3 1.5 copy-start.3
  55.8 1.0 copy-start.1

commit v2 on v0

--- a/solution.py
+++ b/solution.py
@@ -8,6 +8,9 @@
 ROPE = 64
 WIDE_HEAD_SIZE = 128
 NARROW_HEAD_SIZE = 64
+EPS = 1e-06
+ROPE_BASE = 10000.0
+NEG_FILL = -1e30
 
 
 MESH = pl.DeviceIdType.MESH
@@ -280,31 +283,19 @@
     )(*operands)
 
 
-EPS = 1e-06
-ROPE_BASE = 10000.0
-NEG_FILL = -1e30
-
-
-def attend_kernel(sizes, packed, cosine, sine, *refs):
-    groups = len(sizes)
-    queries, key_ws, value_ws = refs[:groups], refs[groups : 2 * groups], refs[2 * groups : 3 * groups]
-    outs = refs[3 * groups : 4 * groups]
-    scratch = refs[4 * groups :]
-    sp = lax.axis_index("sp")
-    tok = cosine.shape[0]
-    latent_width = key_ws[0].shape[0]
-    lanes = packed.shape[1] - latent_width
+def grid(shape):
+    return lax.broadcasted_iota(jnp.int32, shape, 0), lax.broadcasted_iota(jnp.int32, shape, 1)
+
+
+def attend_start(sizes, cosine, sine, queries, widths, scratch):
     half = ROPE // 2
-
-    def grid(shape):
-        return lax.broadcasted_iota(jnp.int32, shape, 0), lax.broadcasted_iota(jnp.int32, shape, 1)
-
+    lanes = cosine.shape[1]
     for g, size in enumerate(sizes):
         plain, turned, peak, total, mixed = scratch[5 * g : 5 * g + 5]
         query = queries[g][...]
         width = query.shape[1]
         for h in range(plain.shape[0]):
-            i, j = grid((width, key_ws[g].shape[1]))
+            i, j = grid((width, widths[g]))
             select = (i == j + h * ROPE) & (j >= h * size) & (j < (h + 1) * size)
             plain[h] = jnp.dot(
                 query, select.astype(jnp.bfloat16), preferred_element_type=jnp.float32
@@ -325,39 +316,42 @@
         total[...] = jnp.zeros_like(total)
         mixed[...] = jnp.zeros_like(mixed)
 
-    def one_block(index, carry):
-        start = pl.ds(pl.multiple_of(index * tok, tok), tok)
-        latent = packed[start, :latent_width]
-        turned_rows = packed[start, latent_width:]
-        i, j = grid((tok, tok))
-        visible = index * tok + j <= sp * tok + i
-        across = (((1,), (1,)), ((), ()))
-        for g, size in enumerate(sizes):
-            plain, turned, peak, total, mixed = scratch[5 * g : 5 * g + 5]
-            factor = (size + ROPE) ** (-0.5)
-            keys = jnp.dot(latent, key_ws[g][...], preferred_element_type=jnp.float32)
-            keys = keys.astype(jnp.bfloat16)
-            values = jnp.dot(latent, value_ws[g][...], preferred_element_type=jnp.float32)
-            values = values.astype(jnp.bfloat16)
-            for h in range(plain.shape[0]):
-                scores = lax.dot_general(
-                    plain[h], keys, across, preferred_element_type=jnp.float32
-                ) + lax.dot_general(
-                    turned[h], turned_rows, across, preferred_element_type=jnp.float32
-                )
-                scores = jnp.where(visible, scores * factor, NEG_FILL)
-                old = peak[h]
-                new = jnp.maximum(old, jnp.max(scores, axis=1, keepdims=True))
-                probs = jnp.where(visible, jnp.exp(scores - new), 0.0)
-                fading = jnp.exp(old - new)
-                peak[h] = new
-                total[h] = total[h] * fading + jnp.sum(probs, axis=1, keepdims=True)
-                mixed[h] = mixed[h] * fading + jnp.dot(
-                    probs.astype(jnp.bfloat16), values, preferred_element_type=jnp.float32
-                )
-        return carry
-
-    lax.fori_loop(0, sp + 1, one_block, 0)
+
+def attend_block(sizes, packed, index, sp, key_ws, value_ws, scratch):
+    latent_width = key_ws[0].shape[0]
+    tok = scratch[0].shape[1]
+    start = pl.ds(pl.multiple_of(index * tok, tok), tok)
+    latent = packed[start, :latent_width]
+    turned_rows = packed[start, latent_width:]
+    i, j = grid((tok, tok))
+    visible = index * tok + j <= sp * tok + i
+    across = (((1,), (1,)), ((), ()))
+    for g, size in enumerate(sizes):
+        plain, turned, peak, total, mixed = scratch[5 * g : 5 * g + 5]
+        factor = (size + ROPE) ** (-0.5)
+        keys = jnp.dot(latent, key_ws[g][...], preferred_element_type=jnp.float32)
+        keys = keys.astype(jnp.bfloat16)
+        values = jnp.dot(latent, value_ws[g][...], preferred_element_type=jnp.float32)
+        values = values.astype(jnp.bfloat16)
+        for h in range(plain.shape[0]):
+            scores = lax.dot_general(
+                plain[h], keys, across, preferred_element_type=jnp.float32
+            ) + lax.dot_general(
+                turned[h], turned_rows, across, preferred_element_type=jnp.float32
+            )
+            scores = jnp.where(visible, scores * factor, NEG_FILL)
+            old = peak[h]
+            new = jnp.maximum(old, jnp.max(scores, axis=1, keepdims=True))
+            probs = jnp.where(visible, jnp.exp(scores - new), 0.0)
+            fading = jnp.exp(old - new)
+            peak[h] = new
+            total[h] = total[h] * fading + jnp.sum(probs, axis=1, keepdims=True)
+            mixed[h] = mixed[h] * fading + jnp.dot(
+                probs.astype(jnp.bfloat16), values, preferred_element_type=jnp.float32
+            )
+
+
+def attend_end(sizes, outs, scratch):
     for g, size in enumerate(sizes):
         plain, turned, peak, total, mixed = scratch[5 * g : 5 * g + 5]
         i, j = grid(outs[g].shape)
@@ -368,8 +362,23 @@
         outs[g][...] = result.astype(jnp.bfloat16)
 
 
-def attend(packed, cosine, sine, queries, key_ws, value_ws, sizes):
-    tok, lanes = cosine.shape
+def attend_kernel(sizes, packed, cosine, sine, *refs):
+    groups = len(sizes)
+    queries, key_ws, value_ws = refs[:groups], refs[groups : 2 * groups], refs[2 * groups : 3 * groups]
+    outs = refs[3 * groups : 4 * groups]
+    scratch = refs[4 * groups :]
+    sp = lax.axis_index("sp")
+    attend_start(sizes, cosine, sine, queries, [w.shape[1] for w in key_ws], scratch)
+
+    def one_block(index, carry):
+        attend_block(sizes, packed, index, sp, key_ws, value_ws, scratch)
+        return carry
+
+    lax.fori_loop(0, sp + 1, one_block, 0)
+    attend_end(sizes, outs, scratch)
+
+
+def attend_scratch(tok, lanes, key_ws, value_ws, sizes):
     scratch = []
     for g, size in enumerate(sizes):
         heads = value_ws[g].shape[1] // size
@@ -380,6 +389,12 @@
             pltpu.VMEM((heads, tok, 1), jnp.float32),
             pltpu.VMEM((heads, tok, value_ws[g].shape[1]), jnp.float32),
         ]
+    return scratch
+
+
+def attend(packed, cosine, sine, queries, key_ws, value_ws, sizes):
+    tok, lanes = cosine.shape
+    scratch = attend_scratch(tok, lanes, key_ws, value_ws, sizes)
     return pl.pallas_call(
         lambda *refs: attend_kernel(sizes, *refs),
         out_shape=[jax.ShapeDtypeStruct((tok, w.shape[1]), jnp.bfloat16) for w in value_ws],
@@ -451,6 +466,652 @@
         pltpu.SemaphoreType.DMA((count,)),
         pltpu.SemaphoreType.DMA,
     ]
+
+
+def layer_kernel(chunks, cap, sizes, *refs):
+    groups = len(sizes)
+    x_ref, cosine, sine = refs[:3]
+    queries, key_ws, value_ws = (refs[3 + k * groups : 3 + (k + 1) * groups] for k in range(3))
+    refs = refs[3 + 3 * groups :]
+    facts_ref, gain_ref, residual_ref = refs[:3]
+    hbm, out_ref, refs = refs[3:11], refs[11], refs[12:]
+    heads_scratch, refs = refs[: 5 * groups], refs[5 * groups :]
+    packed, mixes, refs = refs[0], refs[1 : 1 + groups], refs[1 + groups :]
+    meta, factors, factor_out, stream, x_scr = refs[:5]
+    blk, plane, gbuf, crow, chs, chin, fin = refs[5:12]
+    bsent, bgot, sent, got = refs[12:16]
+    local = refs[16:24]
+    ow, on, sg, su, sd, eg, eu, ed = local
+    smat, som, wcol, hg, hu, aout, ain, spread_act, shg, shu, sact, facc, squares = refs[24:37]
+    refs = refs[37:]
+    wsem, lsend, lrecv, psend_l, precv_l, msend, mrecv, fsend, frecv_f = refs[:9]
+    psend, precv, csend, crecv, gsend, grecv, asend, arecv = refs[9:17]
+    dsend, drecv, frecv, rsend, rrecv, bsend, brecv, esend, erecv, ysend = refs[17:27]
+    z, tp = lax.axis_index("sp"), lax.axis_index("tp")
+    group = lax.axis_index("grp")
+    n_sp, n_tp = lax.axis_size("sp"), lax.axis_size("tp")
+    count = n_sp * n_tp
+    me = z * n_tp + tp
+    rows, width = stream.shape
+    tok = x_ref.shape[0]
+    part = width // chunks
+    hidden_width = eg.shape[0]
+    way = 1 - 2 * (z // 2)
+    f32, bf16 = jnp.float32, jnp.bfloat16
+
+    def cols(q):
+        return pl.ds(pl.multiple_of(q * part, part), part)
+
+    def peer(d):
+        return {"tp": flip(tp, d)}
+
+    def dot(a, b):
+        return jnp.dot(a, b, preferred_element_type=f32)
+
+    def dot_nt(a, b):
+        return lax.dot_general(a, b, (((1,), (1,)), ((), ())), preferred_element_type=f32)
+
+    def dot_tn(a, b):
+        return lax.dot_general(a, b, (((0,), (0,)), ((), ())), preferred_element_type=f32)
+
+    def other(k):
+        return {
+            "sp": lax.rem(z + k // n_tp, n_sp),
+            "tp": lax.rem(tp + lax.rem(k, n_tp), n_tp),
+        }
+
+    def others(step):
+        def one(k, carry):
+            step(k)
+            return carry
+
+        lax.fori_loop(1, count, one, 0)
+
+    barrier = pltpu.get_barrier_semaphore()
+    others(
+        lambda k: pl.semaphore_signal(barrier, inc=1, device_id=other(k), device_id_type=MESH)
+    )
+    pl.semaphore_signal(barrier, inc=1, device_id={"grp": 1 - group}, device_id_type=MESH)
+    landing = [ed.at[0] if k == 7 else local[k] for k in range(8)]
+    loads = [pltpu.make_async_copy(a, b, wsem.at[k]) for k, (a, b) in enumerate(zip(hbm, landing))]
+    for k in (7, 0, 1, 5, 6, 2, 3, 4):
+        loads[k].start()
+    pl.semaphore_wait(barrier, count)
+
+    half = tok // 2
+    mine = lax.rem(tp, 2) * half
+
+    def latent_rows(block, start):
+        return pl.ds(pl.multiple_of(block * tok + start, half), half)
+
+    def latent_out(block, source=None):
+        into = packed.at[latent_rows(block, mine)]
+        source = into if source is None else source
+        return remote(source, into, lsend.at[block], lrecv.at[block], {"sp": z + 1})
+
+    def latent_over(block):
+        at = packed.at[latent_rows(block, mine)]
+        return remote(at, at, psend_l.at[block], precv_l.at[block], peer(1))
+
+    def latent_here(block):
+        at = packed.at[latent_rows(block, half - mine)]
+        remote(at, at, psend_l.at[block], precv_l.at[block], peer(1)).wait_recv()
+
+    @pl.when(z < n_sp - 1)
+    def _():
+        latent_out(z, x_ref.at[pl.ds(pl.multiple_of(mine, half), half)]).start()
+
+    def fact_out(k):
+        return remote(facts_ref, meta.at[me], msend.at[k], mrecv.at[me], other(k))
+
+    def factor_send(k):
+        return remote(factor_out, factors.at[me], fsend.at[k], frecv_f.at[me], other(k))
+
+    others(lambda k: fact_out(k).start())
+    meta[me] = facts_ref[...]
+
+    def down_out(m, q):
+        return remote(
+            ed.at[0, :, cols(q)],
+            ed.at[m, :, cols(q)],
+            esend.at[m, q],
+            erecv.at[m, q],
+            peer(m),
+        )
+
+    def down_on(q):
+        return remote(
+            ed.at[2, :, cols(q)],
+            ed.at[3, :, cols(q)],
+            esend.at[3, q],
+            erecv.at[3, q],
+            peer(1),
+        )
+
+    def down_across(q):
+        at = ed.at[2, :, cols(q)]
+        return remote(at, at, ysend.at[q], erecv.at[2, q], {"grp": 1 - group})
+
+    loads[7].wait()
+    for i in range(chunks // 2):
+        down_out(2, 2 * i + group).start()
+    for q in range(chunks):
+        down_out(1, q).start()
+
+    packed[pl.ds(pl.multiple_of(z * tok, tok), tok)] = x_ref[...]
+    attend_start(sizes, cosine, sine, queries, [w.shape[1] for w in key_ws], heads_scratch)
+    attend_block(sizes, packed, z, z, key_ws, value_ws, heads_scratch)
+
+    def earlier(k, carry):
+        block = z - k
+        remote(
+            packed.at[latent_rows(block, mine)],
+            packed.at[latent_rows(block, mine)],
+            lsend.at[block],
+            lrecv.at[block],
+            peer(1),
+        ).wait_recv()
+
+        @pl.when(z < n_sp - 1)
+        def _():
+            latent_out(block).start()
+
+        latent_over(block).start()
+        latent_here(block)
+        attend_block(sizes, packed, block, z, key_ws, value_ws, heads_scratch)
+        return carry
+
+    lax.fori_loop(1, z + 1, earlier, 0)
+    attend_end(sizes, mixes, heads_scratch)
+
+    def block_out(p, q, k, target, source=None):
+        source = blk.at[p, :, cols(q)] if source is None else source
+        return remote(source, blk.at[p, :, cols(q)], csend.at[k, q], crecv.at[p, q], target)
+
+    def own_out(q, step):
+        return block_out(z, q, (1 - step) // 2, {"sp": z + step}, x_scr.at[:, cols(q)])
+
+    def gather_out(m, q):
+        return remote(
+            x_scr.at[:, cols(q)],
+            plane.at[pl.ds(m * rows, rows), cols(q)],
+            psend.at[m, q],
+            precv.at[m, q],
+            peer(m),
+        )
+
+    def gather_on(q):
+        return remote(
+            plane.at[pl.ds(2 * rows, rows), cols(q)],
+            plane.at[pl.ds(3 * rows, rows), cols(q)],
+            psend.at[3, q],
+            precv.at[3, q],
+            peer(1),
+        )
+
+    def fold_in(sends, gets, send_sem, recv_sem):
+        def fold(d, q, mask):
+            return remote(
+                sends.at[d, :, cols(q)],
+                gets.at[d, :, cols(q)],
+                send_sem.at[d, q],
+                recv_sem.at[d, q],
+                peer(mask),
+            )
+
+        return fold
+
+    first_fold = fold_in(bsent, bgot, bsend, brecv)
+    fold = fold_in(sent, got, rsend, rrecv)
+
+    def projected(d, q):
+        start = pl.ds(pl.multiple_of(flip(tp, d) * rows, rows), rows)
+        return dot(mixes[0][start, :], ow[:, cols(q)]) + dot(mixes[1][start, :], on[:, cols(q)])
+
+    def b1(q):
+        for d in (3, 1):
+            bsent[d, :, cols(q)] = projected(d, q).astype(bf16)
+            first_fold(d, q, 1).start()
+
+    def b2(q):
+        total = projected(2, q)
+        first_fold(3, q, 1).wait_recv()
+        bsent[2, :, cols(q)] = (total + bgot[3, :, cols(q)].astype(f32)).astype(bf16)
+        first_fold(2, q, 2).start()
+
+    def b3(q):
+        total = projected(0, q) + residual_ref[:, cols(q)].astype(f32)
+        first_fold(1, q, 1).wait_recv()
+        total = total + bgot[1, :, cols(q)].astype(f32)
+        first_fold(2, q, 2).wait_recv()
+        total = (total + bgot[2, :, cols(q)].astype(f32)).astype(bf16)
+        stream[:, cols(q)] = total
+        total = total.astype(f32)
+        squares[...] += jnp.sum(total * total, axis=1, keepdims=True)
+        scaled = (total * gain_ref[:, cols(q)]).astype(bf16)
+        x_scr[:, cols(q)] = scaled
+
+        @pl.when(z < n_sp - 1)
+        def _():
+            own_out(q, 1).start()
+
+        @pl.when(z > 0)
+        def _():
+            own_out(q, -1).start()
+
+        gather_out(2, q).start()
+        gather_out(1, q).start()
+        plane[:rows, cols(q)] = scaled
+
+        @pl.when(q < chunks // 2)
+        def _():
+            down_out(2, 2 * q + group).wait_recv()
+            down_across(2 * q + group).start()
+
+    def staged(*stages):
+        def one(q, carry):
+            for lag, stage in enumerate(stages):
+
+                @pl.when((q >= lag) & (q < chunks + lag))
+                def _():
+                    stage(q - lag)
+
+            return carry
+
+        lax.fori_loop(0, chunks + len(stages) - 1, one, 0)
+
+    loads[0].wait()
+    loads[1].wait()
+    squares[...] = jnp.zeros_like(squares)
+    staged(b1, b2, b3)
+    factor = lax.rsqrt(squares[...] * (1.0 / width) + EPS)
+    i, j = grid((rows, factor_out.shape[1]))
+    factor = jnp.sum(jnp.where(i == j, factor, 0.0), axis=0, keepdims=True)
+    factor_out[...] = jnp.broadcast_to(factor, factor_out.shape)
+    others(lambda k: factor_send(k).start())
+    factors[me] = factor_out[...]
+
+    hg[...] = jnp.zeros_like(hg)
+    hu[...] = jnp.zeros_like(hu)
+    shg[...] = jnp.zeros_like(shg)
+    shu[...] = jnp.zeros_like(shu)
+    som[...] = jnp.zeros_like(som)
+    lanes = meta.shape[2]
+    iota = lax.broadcasted_iota(jnp.int32, (cap, lanes), 0)
+
+    def fact_wait(k):
+        source = lax.rem(z + k // n_tp, n_sp) * n_tp + lax.rem(tp + lax.rem(k, n_tp), n_tp)
+        remote(facts_ref, meta.at[source], msend.at[k], mrecv.at[source], peer(1)).wait_recv()
+
+    others(fact_wait)
+
+    def held(p, d):
+        info = meta[p * n_tp + flip(tp, d)]
+        slot = ((z * n_tp + tp) * cap + iota).astype(f32)
+        return info, info[0:1, :] == slot, info[1:2, :] == slot
+
+    for step in range(n_sp):
+        p = lax.rem(z + step, n_sp)
+        for d in range(n_tp):
+            info = meta[p * n_tp + tp]
+            slot = ((z * n_tp + flip(tp, d)) * cap + iota).astype(f32)
+            hit = (info[0:1, :] == slot) | (info[1:2, :] == slot)
+            smat[p, d * cap : (d + 1) * cap, :] = hit.astype(f32)[:, :rows].astype(bf16)
+            info, first, second = held(p, d)
+            weight = jnp.where(first, info[2:3, :], 0.0) + jnp.where(second, info[3:4, :], 0.0)
+            wcol[p, d * cap : (d + 1) * cap, :] = jnp.sum(weight, axis=1, keepdims=True)
+            if not step:
+                hit = (first | second).astype(f32)[:, :rows].astype(bf16)
+                som[d * cap : (d + 1) * cap, d * rows : (d + 1) * rows] = hit
+
+    def piece(p, d, q):
+        return p, pl.ds(d * cap, cap), cols(q)
+
+    def spread_out(p, d, q):
+        at = piece(p, d, q)
+        return remote(gbuf.at[at], crow.at[at], gsend.at[p, d, q], grecv.at[p, d, q], peer(d))
+
+    def c_unit(p, q, k=None, target=None):
+        block_out(p, q, 0, peer(1)).wait_recv()
+        if k is not None:
+            block_out(p, q, k, target).start()
+        picked = dot(smat[p], blk[p, :, cols(q)]).astype(bf16)
+        gbuf[p, :, cols(q)] = picked
+        crow[p, :cap, cols(q)] = picked[:cap]
+        for d in (2, 3, 1):
+            spread_out(p, d, q).start()
+
+    def hidden(p, q):
+        taken = crow[p, :, cols(q)]
+        hg[p] += dot_nt(taken, eg[:, cols(q)])
+        hu[p] += dot_nt(taken, eu[:, cols(q)])
+
+    def h_unit(p, q):
+        for d in (1, 2, 3):
+            spread_out(p, d, q).wait_recv()
+        hidden(p, q)
+
+    def act_out(p, d):
+        at = (p, pl.ds(d * cap, cap))
+        return remote(aout.at[at], ain.at[at], asend.at[p, d], arecv.at[p, d], peer(d))
+
+    def factor_of(p, d):
+        source = p * n_tp + flip(tp, d)
+
+        @pl.when(source != me)
+        def _():
+            remote(
+                factor_out, factors.at[source], fsend.at[0], frecv_f.at[source], peer(1)
+            ).wait_recv()
+
+        return factors[source][0:1, :]
+
+    def silu(gate):
+        return gate / (1.0 + jnp.exp(-gate))
+
+    def activate(p, values=None):
+        for d in range(n_tp):
+            at = pl.ds(d * cap, cap)
+            value = factor_of(p, d) if values is None else values[d]
+            _, first, second = held(p, d)
+            scale = jnp.sum(jnp.where(first | second, value, 0.0), axis=1, keepdims=True)
+            made = silu(hg[p, at, :] * scale) * (hu[p, at, :] * scale) * wcol[p, at, :]
+            made = made.astype(bf16)
+            if d:
+                aout[p, at, :] = made
+                act_out(p, d).start()
+            else:
+                ain[p, at, :] = made
+
+    def mix_in(p):
+        for d in range(n_tp):
+            if d:
+                act_out(p, d).wait_recv()
+            at = pl.ds(d * cap, cap)
+            spread_act[p, d] = dot_tn(smat[p, at, :], ain[p, at, :]).astype(bf16)
+
+    def own_unit(q):
+        gather_out(2, q).wait_recv()
+        gather_on(q).start()
+        gather_out(1, q).wait_recv()
+        gather_on(q).wait_recv()
+        full = plane[:, cols(q)]
+        crow[z, :, cols(q)] = dot(som[...], full).astype(bf16)
+        shg[...] += dot(full, sg[cols(q), :])
+        shu[...] += dot(full, su[cols(q), :])
+        hidden(z, q)
+
+    def own_activate():
+        values = [factor_of(z, d) for d in range(n_tp)]
+        activate(z, values)
+        i, j = grid((rows, lanes))
+        for d in range(n_tp):
+            at = pl.ds(d * rows, rows)
+            scale = jnp.sum(jnp.where(i == j, values[d], 0.0), axis=1, keepdims=True)
+            sact[at, :] = (silu(shg[at, :] * scale) * (shu[at, :] * scale)).astype(bf16)
+
+    def outcome(p, q):
+        total = dot(spread_act[p, 0], ed[0, :, cols(q)])
+        for d in range(1, n_tp):
+            total = total + dot(spread_act[p, d], ed[d, :, cols(q)])
+        return total
+
+    def down_relay(q):
+        @pl.when(lax.rem(q, 2) != group)
+        def _():
+            down_out(2, q).wait_recv()
+
+        down_on(q).start()
+
+    def down_ready(q):
+        down_out(1, q).wait_recv()
+        down_on(q).wait_recv()
+
+    def chain_out(p, q, last, step):
+        into, sem = chin.at[p, :, cols(q)], drecv.at[p, q]
+        if last:
+            side = (1 - step) // 2
+            into, sem = fin.at[side, :, cols(q)], frecv.at[side, q]
+        return remote(chs.at[p, :, cols(q)], into, dsend.at[p, q], sem, {"sp": z + step})
+
+    def d_unit(p, q, incoming, last, step):
+        total = outcome(p, q)
+        if incoming:
+            chain_out(p, q, False, step).wait_recv()
+            total = total + chin[p, :, cols(q)].astype(f32)
+        chs[p, :, cols(q)] = total.astype(bf16)
+        chain_out(p, q, last, step).start()
+
+    def product(d, q):
+        return dot(sact[d * rows : (d + 1) * rows, :], sd[:, cols(q)])
+
+    def rs1(q):
+        for d in (3, 1):
+            sent[d, :, cols(q)] = product(d, q).astype(bf16)
+            fold(d, q, 1).start()
+
+    def rs2(q):
+        total = product(2, q)
+        fold(3, q, 1).wait_recv()
+        sent[2, :, cols(q)] = (total + got[3, :, cols(q)].astype(f32)).astype(bf16)
+        fold(2, q, 2).start()
+
+    def base(q):
+        total = product(0, q) + outcome(z, q) + stream[:, cols(q)].astype(f32)
+        fold(1, q, 1).wait_recv()
+        total = total + got[1, :, cols(q)].astype(f32)
+        fold(2, q, 2).wait_recv()
+        facc[:, cols(q)] = total + got[2, :, cols(q)].astype(f32)
+
+    def arrive(side, q):
+        at = fin.at[side, :, cols(q)]
+        remote(at, at, dsend.at[0, q], frecv.at[side, q], peer(1)).wait_recv()
+        return fin[side, :, cols(q)].astype(f32)
+
+    def run(*steps):
+        def each(q):
+            for step in steps:
+                step(q)
+
+        return each
+
+    def at_first(step):
+        def each(q):
+            @pl.when(q == 0)
+            def _():
+                step()
+
+        return each
+
+    def sends_done(copies):
+        def one(q, carry):
+            for copy in copies(q):
+                copy.wait_send()
+            return carry
+
+        lax.fori_loop(0, chunks, one, 0)
+
+    for k in (5, 6, 2, 3, 4):
+        loads[k].wait()
+
+    is_end = (z == 0) | (z == n_sp - 1)
+
+    @pl.when(is_end)
+    def _():
+        p0, p1, p2 = z + way, z + 2 * way, z + 3 * way
+        staged(run(lambda q: c_unit(p0, q), own_unit), lambda q: h_unit(p0, q))
+        activate(p0)
+        own_activate()
+        staged(
+            run(lambda q: c_unit(p1, q), down_relay),
+            run(
+                at_first(lambda: mix_in(p0)),
+                lambda q: h_unit(p1, q),
+                down_ready,
+                lambda q: d_unit(p0, q, False, True, way),
+            ),
+        )
+        activate(p1)
+        staged(
+            lambda q: c_unit(p2, q),
+            run(
+                at_first(lambda: mix_in(p1)),
+                lambda q: h_unit(p2, q),
+                lambda q: d_unit(p1, q, False, False, way),
+            ),
+        )
+        activate(p2)
+        staged(rs1)
+        mix_in(p2)
+        staged(run(lambda q: d_unit(p2, q, False, False, way), rs2))
+        mix_in(z)
+        staged(base)
+
+        def last(q):
+            out_ref[:, cols(q)] = (facc[:, cols(q)] + arrive((1 + way) // 2, q)).astype(bf16)
+
+        staged(last)
+        sends_done(
+            lambda q: [own_out(q, way)]
+            + [spread_out(p, d, q) for p in (p0, p1, p2) for d in (1, 2, 3)]
+            + [chain_out(p, q, False, way) for p in (p0, p1, p2)]
+        )
+
+    @pl.when(jnp.logical_not(is_end))
+    def _():
+        s0, s1, s2 = z - way, z + way, z + 2 * way
+        ahead, behind = {"sp": z + way}, {"sp": z - way}
+        staged(
+            run(
+                lambda q: c_unit(s0, q, 2, ahead),
+                lambda q: c_unit(s1, q, 3, behind),
+                own_unit,
+            ),
+            run(lambda q: h_unit(s0, q), lambda q: h_unit(s1, q)),
+        )
+        activate(s0)
+        activate(s1)
+        own_activate()
+        staged(
+            run(lambda q: c_unit(s2, q, 4, behind), down_relay),
+            run(lambda q: h_unit(s2, q), down_ready),
+        )
+        activate(s2)
+        mix_in(s1)
+        staged(run(rs1, lambda q: d_unit(s1, q, True, True, way)), rs2)
+        mix_in(s2)
+        mix_in(s0)
+        mix_in(z)
+        staged(
+            run(
+                lambda q: d_unit(s2, q, True, False, way),
+                lambda q: d_unit(s0, q, True, True, -way),
+            ),
+            base,
+        )
+
+        def last(q):
+            total = facc[:, cols(q)] + arrive(0, q) + arrive(1, q)
+            out_ref[:, cols(q)] = total.astype(bf16)
+
+        staged(last)
+        sends_done(
+            lambda q: [own_out(q, way), own_out(q, -way)]
+            + [block_out(s0, q, 2, ahead), block_out(s1, q, 3, behind)]
+            + [block_out(s2, q, 4, behind)]
+            + [spread_out(p, d, q) for p in (s0, s1, s2) for d in (1, 2, 3)]
+            + [chain_out(p, q, False, way) for p in (s0, s1, s2)]
+        )
+
+    sends_done(
+        lambda q: [gather_out(2, q), gather_out(1, q), gather_on(q)]
+        + [down_out(1, q), down_on(q)]
+        + [f(d, q, 1) for f in (fold, first_fold) for d in (3, 1, 2)]
+    )
+    for i in range(chunks // 2):
+        down_out(2, 2 * i + group).wait_send()
+        down_across(2 * i + group).wait_send()
+    for p in range(n_sp):
+        for d in range(1, n_tp):
+            act_out(p, d).wait_send()
+
+    def finish(k):
+        fact_out(k).wait_send()
+        factor_send(k).wait_send()
+
+    others(finish)
+
+    def latents_done(block, carry):
+        @pl.when(z < n_sp - 1)
+        def _():
+            latent_out(block).wait_send()
+
+        @pl.when(block < z)
+        def _():
+            latent_over(block).wait_send()
+
+        return carry
+
+    lax.fori_loop(0, z + 1, latents_done, 0)
+
+
+def layer(near, far, n_sp, n_tp, cap, sizes, chunks=4):
+    groups = len(sizes)
+    rows_packed, cosine = near[:2]
+    key_ws, value_ws = (near[3 + k * groups : 3 + (k + 1) * groups] for k in (1, 2))
+    residual = near[-1]
+    facts = near[-3]
+    tok, lanes = cosine.shape
+    rows, width = residual.shape
+    ow, on, sg, su, sd, eg, eu, ed = far
+    slots = n_tp * cap
+    hidden, share = eg.shape[0], sg.shape[1]
+    bf16, f32 = jnp.bfloat16, jnp.float32
+    count = n_sp * n_tp
+
+    def sems(*shape):
+        return pltpu.SemaphoreType.DMA(shape)
+
+    def half(*shape):
+        return pltpu.VMEM(shape, bf16)
+
+    def full(*shape):
+        return pltpu.VMEM(shape, f32)
+
+    scratch = attend_scratch(tok, lanes, key_ws, value_ws, sizes)
+    scratch += [half(n_sp * tok, rows_packed.shape[1])]
+    scratch += [half(tok, w.shape[1]) for w in value_ws]
+    scratch += [full(count, *facts.shape), full(count, *facts.shape), full(*facts.shape)]
+    scratch += [half(rows, width), half(rows, width)]
+    scratch += [half(n_sp, rows, width), half(n_tp * rows, width)]
+    scratch += [half(n_sp, slots, width)] * 2
+    scratch += [half(n_sp, rows, width)] * 2 + [half(2, rows, width)]
+    scratch += [half(n_tp, rows, width)] * 4
+    scratch += [half(*w.shape) for w in far[:-1]] + [half(n_tp, *ed.shape)]
+    scratch += [half(n_sp, slots, rows), half(slots, n_tp * rows), full(n_sp, slots, 1)]
+    scratch += [full(n_sp, slots, hidden)] * 2
+    scratch += [half(n_sp, slots, hidden)] * 2
+    scratch += [half(n_sp, n_tp, rows, hidden)]
+    scratch += [full(n_tp * rows, share)] * 2 + [half(n_tp * rows, share)]
+    scratch += [full(rows, width), full(rows, 1)]
+    scratch += [sems(8)] + [sems(n_sp)] * 4
+    scratch += [sems(count)] * 4
+    scratch += [sems(n_tp, chunks)] * 2
+    scratch += [sems(5, chunks), sems(n_sp, chunks)]
+    scratch += [sems(n_sp, n_tp, chunks)] * 2
+    scratch += [sems(n_sp, n_tp)] * 2
+    scratch += [sems(n_sp, chunks), sems(n_sp, chunks), sems(2, chunks)]
+    scratch += [sems(n_tp, chunks)] * 6 + [sems(chunks)]
+    return pl.pallas_call(
+        lambda *refs: layer_kernel(chunks, cap, sizes, *refs),
+        out_shape=jax.ShapeDtypeStruct((rows, width), bf16),
+        in_specs=[VMEM] * len(near) + [pl.BlockSpec(memory_space=pl.ANY)] * len(far),
+        out_specs=VMEM,
+        scratch_shapes=scratch,
+        compiler_params=pltpu.CompilerParams(
+            collective_id=4, has_side_effects=True, vmem_limit_bytes=60 << 20
+        ),
+    )(*near, *far)
 
 
 def rms_scale(values, gain):
@@ -499,24 +1160,10 @@
         jnp.dot(rope_key, same, preferred_element_type=jnp.float32) * cosine
         + jnp.dot(rope_key, cross.astype(jnp.bfloat16), preferred_element_type=jnp.float32) * sine
     ).astype(jnp.bfloat16)
-    packed = spread(jnp.concatenate([normed_latent, turned_key], axis=1), n_sp, n_tp)
-    wide_mix, narrow_mix = attend(
-        packed,
-        cosine,
-        sine,
-        (wide_query, narrow_query),
-        (wide_key_weight, narrow_key_weight),
-        (wide_value_weight, narrow_value_weight),
-        (WIDE_HEAD_SIZE, NARROW_HEAD_SIZE),
-    )
-    (projected,) = dot_scatter((wide_mix, narrow_mix), (out_wide, out_narrow), n_tp, 2)
-    stream = (residual.astype(jnp.float32) + projected).astype(jnp.bfloat16)
-    normed = rms_scale(stream.astype(jnp.float32), ffn_gain).astype(jnp.bfloat16)
     rows_here, top_count = routes.shape
     local_experts = expert_gate.shape[0]
     experts_all = local_experts * lax.axis_size(("sp", "tp"))
     capacity = max(2, 2 * top_count * rows_here // experts_all)
-    model_width = normed.shape[1]
     flat_routes = routes.reshape(-1)
     assigned = flat_routes.shape[0]
     choose = (flat_routes[:, None] == jnp.arange(experts_all, dtype=jnp.int32)[None, :]).astype(
@@ -526,6 +1173,29 @@
     earlier = jnp.dot(lower_mask, choose, precision=lax.Precision.HIGHEST)
     slots = jnp.sum(earlier * choose, axis=1).astype(jnp.int32)
     target = flat_routes * capacity + slots
+    by_choice = target.reshape(rows_here, top_count)
+    planes = n_sp == 4 and n_tp == 4 and local_experts == 1 and capacity % 16 == 0
+    fused = planes and top_count == 2 and rows_here <= 128 and lax.axis_size("grp") == 2
+    rows_packed = jnp.concatenate([normed_latent, turned_key], axis=1)
+    queries = (wide_query, narrow_query)
+    key_ws = (wide_key_weight, narrow_key_weight)
+    value_ws = (wide_value_weight, narrow_value_weight)
+    sizes = (WIDE_HEAD_SIZE, NARROW_HEAD_SIZE)
+    if fused:
+        spare = (-rows_here) % 128
+        facts = jnp.concatenate([by_choice.astype(jnp.float32).T, route_weights.T], axis=0)
+        facts = jnp.pad(facts, ((0, 4), (0, spare)), constant_values=-1.0)
+        near = (rows_packed, cosine, sine, *queries, *key_ws, *value_ws)
+        near += (facts, ffn_gain[None, :], residual)
+        far = (out_wide, out_narrow, shared_gate, shared_up, shared_down)
+        far += (expert_gate[0].T, expert_up[0].T, expert_down[0])
+        return layer(near, far, n_sp, n_tp, capacity, sizes)
+    packed = spread(rows_packed, n_sp, n_tp)
+    wide_mix, narrow_mix = attend(packed, cosine, sine, queries, key_ws, value_ws, sizes)
+    (projected,) = dot_scatter((wide_mix, narrow_mix), (out_wide, out_narrow), n_tp, 2)
+    stream = (residual.astype(jnp.float32) + projected).astype(jnp.bfloat16)
+    normed = rms_scale(stream.astype(jnp.float32), ffn_gain).astype(jnp.bfloat16)
+    model_width = normed.shape[1]
     send_map = jnp.any(
         target.reshape(rows_here, top_count)[None, :, :]
         == jnp.arange(experts_all * capacity, dtype=jnp.int32)[:, None, None],
@@ -553,7 +1223,6 @@
         (active,), (shared_down,), n_tp, 3, finished.reshape(outgoing.shape)
     )
     slot_rows = returned.reshape(experts_all * capacity, model_width)
-    by_choice = target.reshape(rows_here, top_count)
     routed = jnp.zeros((rows_here, model_width), jnp.float32)
     for choice in range(top_count):
         hot = by_choice[:, choice : choice + 1] == jnp.arange(experts_all * capacity)[None, :]

time: 189 us -> 131 us (0.69)
  Pallas kernels: 160 us -> 120 us
  matrix products: 21.1 us -> 1.21 us
  local copies, waits for them, and re-layouts: 0.67 us -> 2.99 us
    pallas_call x5 -> x1, Pallas kernels: 160 us -> 120 us  [layer(): pl.pallas_call(lambda *refs: layer_kernel(chunks, cap, sizes, *refs), out...]
    dot_general x7 -> x0, matrix products: 18.2 us -> none  [the longest x1 5.86 us: body(): jnp.einsum('sxcf,xfd->sxcd', active, expert_down, preferred_element_type=...]
    unnamed x23 -> x4, local copies, waits for them, and re-layouts: 0.31 us -> 2.64 us
where the time goes in v2:
time: 131 us
  Pallas kernels  120 us (92%)
  other arithmetic  6.17 us (5%)
  local copies, waits for them, and re-layouts  2.99 us (2%)
    pallas_call x1, Pallas kernels, layer(): pl.pallas_call(lambda *refs: layer_kernel(chunks, cap, sizes, *refs), out...  120 us
    unnamed x4, local copies, waits for them, and re-layouts  2.64 us

profile of v2, /device:TPU:0, one launch (start us, length us, event | category | flops | bytes accessed | tf_op | source)
XLA Modules:
  0.0 130.6 jit_solution(5075671328557490105)
XLA Ops:
  0.0 0.0 copy-start
  0.0 1.1 fusion.5
  1.1 0.8 copy.28
  1.9 0.1 eq.62
  2.0 0.2 fusion.4
  2.2 0.1 convert_element_type.56
  2.4 0.1 copy.29
  2.4 0.7 convert_bitcast_fusion
  3.1 1.3 select_maximum_fusion.refs_9_
  4.4 0.0 copy-done
  4.4 0.5 fusion.2
  5.0 0.5 fusion.3
  5.5 1.2 multiply_sine_fusion
  6.7 1.1 fusion.7
  7.8 0.8 pad_maximum_fusion.refs_0_
  8.6 120.2 %shard_map.199 = bf16[64,4096]{1,0:T(8,128)(2,1)} custom-call(bf16[256,640]{1,0:T(8,128)(2,1)} %pad_maximum_fusion.refs_0_, f32[256,128]{1,0:T(8,128)} %get-tuple-element.6.refs_1_, f32[256,128]{1,0:T(8,128)} %get-tuple-element.5.refs_2_, bf16[256,384]{1,0:T(8,128)(2,1)} %refs_3_.1, bf16[256,256]{1,0:T(8,128)(2,1)} %refs_4_.1, bf16[512,256]{1,0:T(8,128)(2,1)} %refs_5_.1, ...), custom_call_target="tpu_custom_call" | custom-call | tf_op jit(solution)/shard_map/pallas_call | solution.py:1105
  128.7 1.9 %copy.33 = bf16[64,4096]{1,0:T(8,128)(2,1)} copy(bf16[64,4096]{1,0:T(8,128)(2,1)} %shard_map.199) | data formatting | bytes 1048576
  (6 shorter events, 0.0 us)
Async XLA Ops:
  0.0 4.4 %copy-start = (bf16[256,64]{0,1:T(8,128)(2,1)S(1)}, bf16[256,64]{0,1:T(8,128)(2,1)}, u32[]{:S(2)}) copy-start(bf16[256,64]{0,1:T(8,128)(2,1)} %param.22) | copy-start | bytes 98308

commit v3 on v2

--- a/solution.py
+++ b/solution.py
@@ -1,5 +1,6 @@
 import jax
 import jax.numpy as jnp
+import numpy as np
 from jax import lax
 from jax.experimental import pallas as pl
 from jax.experimental.pallas import tpu as pltpu
@@ -468,14 +469,102 @@
     ]
 
 
+def turn(straight, crossed, cosine, sine):
+    return (straight * cosine + crossed * sine).astype(jnp.bfloat16)
+
+
+def turn_picks(height, lanes, base):
+    half = ROPE // 2
+    i, j = grid((height, lanes))
+    same = ((i == j + base) & (j < ROPE)).astype(jnp.float32)
+    upper = ((i == j + base + half) & (j < half)).astype(jnp.float32)
+    lower = ((i == j + base - half) & (j >= half) & (j < ROPE)).astype(jnp.float32)
+    return same.astype(jnp.bfloat16), (lower - upper).astype(jnp.bfloat16)
+
+
+class Heads:
+    def __init__(self, sizes, widths, refs):
+        self.sizes, self.widths = sizes, widths
+        self.joined, self.peak, self.total, self.mixed, self.turned_ws = refs
+        self.list = []
+        row = 0
+        for g, size in enumerate(sizes):
+            for h in range(widths[g] // size):
+                self.list.append((g, h, size, row))
+                row += size
+
+    def start(self, queries, value_ws, cosine, sine):
+        lanes = cosine.shape[1]
+        cosine, sine = cosine[...], sine[...]
+        for n, (g, h, size, row) in enumerate(self.list):
+            query = queries[g][...]
+            i, j = grid((query.shape[1], lanes))
+            base = h * (size + ROPE)
+            start = h * size % lanes
+            select = (i == j - start + base) & (j >= start) & (j < start + size)
+            self.joined[n, :, :lanes] = jnp.dot(
+                query, select.astype(jnp.bfloat16), preferred_element_type=jnp.float32
+            ).astype(jnp.bfloat16)
+            same, cross = turn_picks(query.shape[1], lanes, base + size)
+            straight = jnp.dot(query, same, preferred_element_type=jnp.float32)
+            crossed = jnp.dot(query, cross, preferred_element_type=jnp.float32)
+            self.joined[n, :, lanes:] = turn(straight, crossed, cosine, sine)
+        row = 0
+        for weight in value_ws:
+            self.turned_ws[row : row + weight.shape[1], :] = weight[...].T
+            row += weight.shape[1]
+        self.peak[...] = jnp.full_like(self.peak, NEG_FILL)
+        self.total[...] = jnp.zeros_like(self.total)
+        self.mixed[...] = jnp.zeros_like(self.mixed)
+
+    def block(self, latent, turned_rows, key_ws, diagonal):
+        lanes = turned_rows.shape[1]
+        across = (((1,), (1,)), ((), ()))
+        bf16, f32 = jnp.bfloat16, jnp.float32
+        keys = [jnp.dot(latent, w[...], preferred_element_type=f32).astype(bf16) for w in key_ws]
+        values = lax.dot_general(
+            self.turned_ws[...], latent, across, preferred_element_type=f32
+        ).astype(bf16)
+        for n, (g, h, size, row) in enumerate(self.list):
+            scale = (size + ROPE) ** (-0.5) * 1.4426950408889634
+            start = h * size // lanes * lanes
+            joined = jnp.concatenate([keys[g][:, start : start + lanes], turned_rows], axis=1)
+            scores = lax.dot_general(joined, self.joined[n], across, preferred_element_type=f32)
+            if diagonal:
+                i, j = grid(scores.shape)
+                scores = jnp.where(i <= j, scores, NEG_FILL)
+            old = self.peak[n : n + 1, :]
+            new = jnp.maximum(old, jnp.max(scores, axis=0, keepdims=True))
+            probs = jnp.exp2((scores - new) * scale)
+            fading = jnp.exp2((old - new) * scale)
+            self.peak[n : n + 1, :] = new
+            self.total[n : n + 1, :] = self.total[n : n + 1, :] * fading + jnp.sum(
+                probs, axis=0, keepdims=True
+            )
+            at = slice(row, row + size)
+            self.mixed[at, :] = self.mixed[at, :] * fading + jnp.dot(
+                values[at, :], probs.astype(bf16), preferred_element_type=f32
+            )
+
+    def end(self, outs):
+        for n, (g, h, size, row) in enumerate(self.list):
+            at = slice(row, row + size)
+            self.mixed[at, :] = self.mixed[at, :] / self.total[n : n + 1, :]
+        row = 0
+        for out in outs:
+            out[...] = self.mixed[row : row + out.shape[1], :].T.astype(jnp.bfloat16)
+            row += out.shape[1]
+
+
 def layer_kernel(chunks, cap, sizes, *refs):
     groups = len(sizes)
-    x_ref, cosine, sine = refs[:3]
+    latent_ref, rope_ref, latent_gain = refs[:3]
     queries, key_ws, value_ws = (refs[3 + k * groups : 3 + (k + 1) * groups] for k in range(3))
     refs = refs[3 + 3 * groups :]
-    facts_ref, gain_ref, residual_ref = refs[:3]
-    hbm, out_ref, refs = refs[3:11], refs[11], refs[12:]
-    heads_scratch, refs = refs[: 5 * groups], refs[5 * groups :]
+    routes_ref, weights_ref, gain_ref, residual_ref = refs[:4]
+    hbm, tables, out_ref, refs = refs[4:12], refs[12:14], refs[14], refs[15:]
+    heads = Heads(sizes, [w.shape[1] for w in value_ws], refs[:5])
+    cosine, sine, facts_ref, refs = refs[5], refs[6], refs[7], refs[8:]
     packed, mixes, refs = refs[0], refs[1 : 1 + groups], refs[1 + groups :]
     meta, factors, factor_out, stream, x_scr = refs[:5]
     blk, plane, gbuf, crow, chs, chin, fin = refs[5:12]
@@ -493,7 +582,8 @@
     count = n_sp * n_tp
     me = z * n_tp + tp
     rows, width = stream.shape
-    tok = x_ref.shape[0]
+    tok = latent_ref.shape[0]
+    latent_width = latent_ref.shape[1]
     part = width // chunks
     hidden_width = eg.shape[0]
     way = 1 - 2 * (z // 2)
@@ -534,8 +624,36 @@
     pl.semaphore_signal(barrier, inc=1, device_id={"grp": 1 - group}, device_id_type=MESH)
     landing = [ed.at[0] if k == 7 else local[k] for k in range(8)]
     loads = [pltpu.make_async_copy(a, b, wsem.at[k]) for k, (a, b) in enumerate(zip(hbm, landing))]
+    own_rows = pl.ds(pl.multiple_of(z * tok, tok), tok)
+    tables = [
+        pltpu.make_async_copy(a.at[own_rows], b, wsem.at[8 + k])
+        for k, (a, b) in enumerate(zip(tables, (cosine, sine)))
+    ]
+    for table in tables:
+        table.start()
     for k in (7, 0, 1, 5, 6, 2, 3, 4):
         loads[k].start()
+
+    latent = latent_ref[...].astype(f32)
+    latent = rms_scale(latent, latent_gain[...])
+    packed[own_rows, :latent_width] = latent.astype(bf16)
+    firsts = routes_ref[...].astype(f32)
+    facts_ref[...] = jnp.full_like(facts_ref, -1.0)
+    i, j = grid((rows, rows))
+    named = [firsts[k : k + 1, :] for k in range(2)]
+    columns = [
+        jnp.sum(jnp.where(i == j, name, 0.0), axis=1, keepdims=True) for name in named
+    ]
+    for k in range(2):
+        before = [((column == named[k]) & (i < j)).astype(f32) for column in columns]
+        slot = jnp.sum(before[0] + before[1], axis=0, keepdims=True)
+        facts_ref[k : k + 1, :rows] = named[k] * cap + slot
+    facts_ref[2:4, :rows] = weights_ref[...]
+    same, cross = turn_picks(rope_ref.shape[0], cosine.shape[1], 0)
+    straight, crossed = dot_tn(rope_ref[...], same), dot_tn(rope_ref[...], cross)
+    for table in tables:
+        table.wait()
+    packed[own_rows, latent_width:] = turn(straight, crossed, cosine[...], sine[...])
     pl.semaphore_wait(barrier, count)
 
     half = tok // 2
@@ -544,10 +662,9 @@
     def latent_rows(block, start):
         return pl.ds(pl.multiple_of(block * tok + start, half), half)
 
-    def latent_out(block, source=None):
+    def latent_out(block):
         into = packed.at[latent_rows(block, mine)]
-        source = into if source is None else source
-        return remote(source, into, lsend.at[block], lrecv.at[block], {"sp": z + 1})
+        return remote(into, into, lsend.at[block], lrecv.at[block], {"sp": z + 1})
 
     def latent_over(block):
         at = packed.at[latent_rows(block, mine)]
@@ -559,7 +676,7 @@
 
     @pl.when(z < n_sp - 1)
     def _():
-        latent_out(z, x_ref.at[pl.ds(pl.multiple_of(mine, half), half)]).start()
+        latent_out(z).start()
 
     def fact_out(k):
         return remote(facts_ref, meta.at[me], msend.at[k], mrecv.at[me], other(k))
@@ -598,9 +715,13 @@
     for q in range(chunks):
         down_out(1, q).start()
 
-    packed[pl.ds(pl.multiple_of(z * tok, tok), tok)] = x_ref[...]
-    attend_start(sizes, cosine, sine, queries, [w.shape[1] for w in key_ws], heads_scratch)
-    attend_block(sizes, packed, z, z, key_ws, value_ws, heads_scratch)
+    heads.start(queries, value_ws, cosine, sine)
+
+    def attend_rows(block, diagonal):
+        at = pl.ds(pl.multiple_of(block * tok, tok), tok)
+        heads.block(packed[at, :latent_width], packed[at, latent_width:], key_ws, diagonal)
+
+    attend_rows(z, True)
 
     def earlier(k, carry):
         block = z - k
@@ -618,11 +739,11 @@
 
         latent_over(block).start()
         latent_here(block)
-        attend_block(sizes, packed, block, z, key_ws, value_ws, heads_scratch)
+        attend_rows(block, False)
         return carry
 
     lax.fori_loop(1, z + 1, earlier, 0)
-    attend_end(sizes, mixes, heads_scratch)
+    heads.end(mixes)
 
     def block_out(p, q, k, target, source=None):
         source = blk.at[p, :, cols(q)] if source is None else source
@@ -699,8 +820,6 @@
         def _():
             own_out(q, -1).start()
 
-        gather_out(2, q).start()
-        gather_out(1, q).start()
         plane[:rows, cols(q)] = scaled
 
         @pl.when(q < chunks // 2)
@@ -719,17 +838,6 @@
             return carry
 
         lax.fori_loop(0, chunks + len(stages) - 1, one, 0)
-
-    loads[0].wait()
-    loads[1].wait()
-    squares[...] = jnp.zeros_like(squares)
-    staged(b1, b2, b3)
-    factor = lax.rsqrt(squares[...] * (1.0 / width) + EPS)
-    i, j = grid((rows, factor_out.shape[1]))
-    factor = jnp.sum(jnp.where(i == j, factor, 0.0), axis=0, keepdims=True)
-    factor_out[...] = jnp.broadcast_to(factor, factor_out.shape)
-    others(lambda k: factor_send(k).start())
-    factors[me] = factor_out[...]
 
     hg[...] = jnp.zeros_like(hg)
     hu[...] = jnp.zeros_like(hu)
@@ -830,6 +938,10 @@
             at = pl.ds(d * cap, cap)
             spread_act[p, d] = dot_tn(smat[p, at, :], ain[p, at, :]).astype(bf16)
 
+    def own_spread(q):
+        gather_out(2, q).start()
+        gather_out(1, q).start()
+
     def own_unit(q):
         gather_out(2, q).wait_recv()
         gather_on(q).start()
@@ -923,6 +1035,14 @@
 
         return each
 
+    def at_odd(first):
+        def each(q):
+            @pl.when(lax.rem(q, 2) == 1)
+            def _():
+                own_spread(first + q // 2)
+
+        return each
+
     def sends_done(copies):
         def one(q, carry):
             for copy in copies(q):
@@ -931,39 +1051,73 @@
 
         lax.fori_loop(0, chunks, one, 0)
 
-    for k in (5, 6, 2, 3, 4):
+    loads[0].wait()
+    loads[1].wait()
+    squares[...] = jnp.zeros_like(squares)
+    is_end = (z == 0) | (z == n_sp - 1)
+    ahead, behind = {"sp": z + way}, {"sp": z - way}
+
+    def c_first(q):
+        @pl.when(is_end)
+        def _():
+            c_unit(z + way, q)
+
+        @pl.when(jnp.logical_not(is_end))
+        def _():
+            c_unit(z - way, q, 2, ahead)
+            c_unit(z + way, q, 3, behind)
+
+    def h_first(q):
+        @pl.when(is_end)
+        def _():
+            h_unit(z + way, q)
+
+        @pl.when(jnp.logical_not(is_end))
+        def _():
+            h_unit(z - way, q)
+            h_unit(z + way, q)
+
+    for k in (5, 6):
         loads[k].wait()
-
-    is_end = (z == 0) | (z == n_sp - 1)
+    staged(b1, b2, b3, c_first, h_first)
+    factor = lax.rsqrt(squares[...] * (1.0 / width) + EPS)
+    i, j = grid((rows, factor_out.shape[1]))
+    factor = jnp.sum(jnp.where(i == j, factor, 0.0), axis=0, keepdims=True)
+    factor_out[...] = jnp.broadcast_to(factor, factor_out.shape)
+    others(lambda k: factor_send(k).start())
+    factors[me] = factor_out[...]
+
+    for k in (2, 3, 4):
+        loads[k].wait()
 
     @pl.when(is_end)
     def _():
         p0, p1, p2 = z + way, z + 2 * way, z + 3 * way
-        staged(run(lambda q: c_unit(p0, q), own_unit), lambda q: h_unit(p0, q))
         activate(p0)
-        own_activate()
         staged(
-            run(lambda q: c_unit(p1, q), down_relay),
+            run(lambda q: c_unit(p1, q), down_relay, at_odd(0)),
             run(
                 at_first(lambda: mix_in(p0)),
-                lambda q: h_unit(p1, q),
                 down_ready,
                 lambda q: d_unit(p0, q, False, True, way),
+                lambda q: h_unit(p1, q),
             ),
         )
         activate(p1)
         staged(
-            lambda q: c_unit(p2, q),
+            run(lambda q: c_unit(p2, q), at_odd(chunks // 2)),
             run(
                 at_first(lambda: mix_in(p1)),
+                lambda q: d_unit(p1, q, False, False, way),
                 lambda q: h_unit(p2, q),
-                lambda q: d_unit(p1, q, False, False, way),
             ),
         )
         activate(p2)
-        staged(rs1)
         mix_in(p2)
-        staged(run(lambda q: d_unit(p2, q, False, False, way), rs2))
+        staged(lambda q: d_unit(p2, q, False, False, way))
+        staged(own_unit)
+        own_activate()
+        staged(rs1, rs2)
         mix_in(z)
         staged(base)
 
@@ -980,34 +1134,27 @@
     @pl.when(jnp.logical_not(is_end))
     def _():
         s0, s1, s2 = z - way, z + way, z + 2 * way
-        ahead, behind = {"sp": z + way}, {"sp": z - way}
-        staged(
-            run(
-                lambda q: c_unit(s0, q, 2, ahead),
-                lambda q: c_unit(s1, q, 3, behind),
-                own_unit,
-            ),
-            run(lambda q: h_unit(s0, q), lambda q: h_unit(s1, q)),
-        )
         activate(s0)
         activate(s1)
-        own_activate()
         staged(
             run(lambda q: c_unit(s2, q, 4, behind), down_relay),
             run(lambda q: h_unit(s2, q), down_ready),
         )
+        staged(own_spread)
         activate(s2)
         mix_in(s1)
-        staged(run(rs1, lambda q: d_unit(s1, q, True, True, way)), rs2)
+        staged(run(own_unit, lambda q: d_unit(s1, q, True, True, way)))
+        own_activate()
         mix_in(s2)
         mix_in(s0)
+        staged(rs1, rs2)
         mix_in(z)
         staged(
             run(
                 lambda q: d_unit(s2, q, True, False, way),
                 lambda q: d_unit(s0, q, True, True, -way),
+                base,
             ),
-            base,
         )
 
         def last(q):
@@ -1055,13 +1202,21 @@
     lax.fori_loop(0, z + 1, latents_done, 0)
 
 
+def rotary_tables(tokens, lanes):
+    half = ROPE // 2
+    lane = np.arange(lanes) % half
+    inverse = np.float32(ROPE_BASE) ** (-lane.astype(np.float32) * np.float32(2.0 / ROPE))
+    angles = np.arange(tokens, dtype=np.float32)[:, None] * inverse.astype(np.float32)[None, :]
+    return jnp.asarray(np.cos(angles)), jnp.asarray(np.sin(angles))
+
+
 def layer(near, far, n_sp, n_tp, cap, sizes, chunks=4):
     groups = len(sizes)
-    rows_packed, cosine = near[:2]
+    tok, latent_width = near[0].shape
     key_ws, value_ws = (near[3 + k * groups : 3 + (k + 1) * groups] for k in (1, 2))
     residual = near[-1]
-    facts = near[-3]
-    tok, lanes = cosine.shape
+    lanes = ROPE + -ROPE % 128
+    tables = rotary_tables(n_sp * tok, lanes)
     rows, width = residual.shape
     ow, on, sg, su, sd, eg, eu, ed = far
     slots = n_tp * cap
@@ -1078,10 +1233,15 @@
     def full(*shape):
         return pltpu.VMEM(shape, f32)
 
-    scratch = attend_scratch(tok, lanes, key_ws, value_ws, sizes)
-    scratch += [half(n_sp * tok, rows_packed.shape[1])]
+    depth = sum(w.shape[1] for w in value_ws)
+    number = sum(w.shape[1] // size for w, size in zip(value_ws, sizes))
+    fact_shape = (8, rows + -rows % 128)
+    scratch = [half(number, tok, 2 * lanes), full(-(-number // 8) * 8, tok)]
+    scratch += [full(-(-number // 8) * 8, tok), full(depth, tok), half(depth, latent_width)]
+    scratch += [full(tok, lanes), full(tok, lanes), full(*fact_shape)]
+    scratch += [half(n_sp * tok, latent_width + lanes)]
     scratch += [half(tok, w.shape[1]) for w in value_ws]
-    scratch += [full(count, *facts.shape), full(count, *facts.shape), full(*facts.shape)]
+    scratch += [full(count, *fact_shape), full(count, *fact_shape), full(*fact_shape)]
     scratch += [half(rows, width), half(rows, width)]
     scratch += [half(n_sp, rows, width), half(n_tp * rows, width)]
     scratch += [half(n_sp, slots, width)] * 2
@@ -1094,7 +1254,7 @@
     scratch += [half(n_sp, n_tp, rows, hidden)]
     scratch += [full(n_tp * rows, share)] * 2 + [half(n_tp * rows, share)]
     scratch += [full(rows, width), full(rows, 1)]
-    scratch += [sems(8)] + [sems(n_sp)] * 4
+    scratch += [sems(10)] + [sems(n_sp)] * 4
     scratch += [sems(count)] * 4
     scratch += [sems(n_tp, chunks)] * 2
     scratch += [sems(5, chunks), sems(n_sp, chunks)]
@@ -1105,13 +1265,13 @@
     return pl.pallas_call(
         lambda *refs: layer_kernel(chunks, cap, sizes, *refs),
         out_shape=jax.ShapeDtypeStruct((rows, width), bf16),
-        in_specs=[VMEM] * len(near) + [pl.BlockSpec(memory_space=pl.ANY)] * len(far),
+        in_specs=[VMEM] * len(near) + [pl.BlockSpec(memory_space=pl.ANY)] * (len(far) + 2),
         out_specs=VMEM,
         scratch_shapes=scratch,
         compiler_params=pltpu.CompilerParams(
             collective_id=4, has_side_effects=True, vmem_limit_bytes=60 << 20
         ),
-    )(*near, *far)
+    )(*near, *far, *tables)
 
 
 def rms_scale(values, gain):
@@ -1145,6 +1305,21 @@
     seq_index = lax.axis_index("sp")
     own_pos = seq_index * tok_dev + jnp.arange(tok_dev, dtype=jnp.int32)
     n_sp, n_tp = lax.axis_size("sp"), lax.axis_size("tp")
+    rows_here, top_count = routes.shape
+    local_experts = expert_gate.shape[0]
+    experts_all = local_experts * lax.axis_size(("sp", "tp"))
+    capacity = max(2, 2 * top_count * rows_here // experts_all)
+    queries = (wide_query, narrow_query)
+    key_ws = (wide_key_weight, narrow_key_weight)
+    value_ws = (wide_value_weight, narrow_value_weight)
+    sizes = (WIDE_HEAD_SIZE, NARROW_HEAD_SIZE)
+    planes = n_sp == 4 and n_tp == 4 and local_experts == 1 and capacity % 16 == 0
+    if planes and top_count == 2 and rows_here <= 128 and lax.axis_size("grp") == 2:
+        near = (latent, rope_key.T, latent_norm_scale[None, :], *queries, *key_ws, *value_ws)
+        near += (routes.T, route_weights.T, ffn_gain[None, :], residual)
+        far = (out_wide, out_narrow, shared_gate, shared_up, shared_down)
+        far += (expert_gate[0].T, expert_up[0].T, expert_down[0])
+        return layer(near, far, n_sp, n_tp, capacity, sizes)
     normed_latent = rms_scale(latent.astype(jnp.float32), latent_norm_scale).astype(jnp.bfloat16)
     half = ROPE // 2
     lane = jnp.arange(ROPE + -ROPE % 128, dtype=jnp.int32)
@@ -1160,10 +1335,6 @@
         jnp.dot(rope_key, same, preferred_element_type=jnp.float32) * cosine
         + jnp.dot(rope_key, cross.astype(jnp.bfloat16), preferred_element_type=jnp.float32) * sine
     ).astype(jnp.bfloat16)
-    rows_here, top_count = routes.shape
-    local_experts = expert_gate.shape[0]
-    experts_all = local_experts * lax.axis_size(("sp", "tp"))
-    capacity = max(2, 2 * top_count * rows_here // experts_all)
     flat_routes = routes.reshape(-1)
     assigned = flat_routes.shape[0]
     choose = (flat_routes[:, None] == jnp.arange(experts_all, dtype=jnp.int32)[None, :]).astype(
@@ -1174,22 +1345,7 @@
     slots = jnp.sum(earlier * choose, axis=1).astype(jnp.int32)
     target = flat_routes * capacity + slots
     by_choice = target.reshape(rows_here, top_count)
-    planes = n_sp == 4 and n_tp == 4 and local_experts == 1 and capacity % 16 == 0
-    fused = planes and top_count == 2 and rows_here <= 128 and lax.axis_size("grp") == 2
     rows_packed = jnp.concatenate([normed_latent, turned_key], axis=1)
-    queries = (wide_query, narrow_query)
-    key_ws = (wide_key_weight, narrow_key_weight)
-    value_ws = (wide_value_weight, narrow_value_weight)
-    sizes = (WIDE_HEAD_SIZE, NARROW_HEAD_SIZE)
-    if fused:
-        spare = (-rows_here) % 128
-        facts = jnp.concatenate([by_choice.astype(jnp.float32).T, route_weights.T], axis=0)
-        facts = jnp.pad(facts, ((0, 4), (0, spare)), constant_values=-1.0)
-        near = (rows_packed, cosine, sine, *queries, *key_ws, *value_ws)
-        near += (facts, ffn_gain[None, :], residual)
-        far = (out_wide, out_narrow, shared_gate, shared_up, shared_down)
-        far += (expert_gate[0].T, expert_up[0].T, expert_down[0])
-        return layer(near, far, n_sp, n_tp, capacity, sizes)
     packed = spread(rows_packed, n_sp, n_tp)
     wide_mix, narrow_mix = attend(packed, cosine, sine, queries, key_ws, value_ws, sizes)
     (projected,) = dot_scatter((wide_mix, narrow_mix), (out_wide, out_narrow), n_tp, 2)

time: 131 us -> 122 us (0.931)
  other arithmetic: 6.17 us -> 0 us
    concatenate x2 -> x0, other arithmetic: 2.03 us -> none  [the longest x1 1.28 us: body(): jnp.concatenate([by_choice.astype(jnp.float32).T, route_weights.T], axis=0)]
    unnamed x4 -> x1, local copies, waits for them, and re-layouts: 2.64 us -> 1.87 us
where the time goes in v3:
time: 122 us
  Pallas kernels  120 us (98%)
  local copies, waits for them, and re-layouts  1.87 us (2%)
    pallas_call x1, Pallas kernels, layer(): pl.pallas_call(lambda *refs: layer_kernel(chunks, cap, sizes, *refs), out...  120 us

profile of v3, /device:TPU:0, one launch (start us, length us, event | category | flops | bytes accessed | tf_op | source)
XLA Modules:
  0.0 121.8 jit_solution(14639180195962443262)
XLA Ops:
  0.0 120.0 %shard_map.217 = bf16[64,4096]{1,0:T(8,128)(2,1)} custom-call(bf16[256,512]{1,0:T(8,128)(2,1)} %refs_0_.1, bf16[64,256]{1,0:T(8,128)(2,1)} %bitcast.15, f32[1,512]{1,0:T(1,128)} %bitcast.17, bf16[256,384]{1,0:T(8,128)(2,1)} %refs_3_.1, bf16[256,256]{1,0:T(8,128)(2,1)} %refs_4_.1, bf16[512,256]{1,0:T(8,128)(2,1)} %refs_5_.1, bf16[512,128]{1,0:T(8,128)(2,1)} %refs_6_.1, ...), custom_call_target="tpu_custom_call" | custom-call | tf_op jit(solution)/shard_map/pallas_call | solution.py:1265
  120.0 1.9 %copy.25 = bf16[64,4096]{1,0:T(8,128)(2,1)} copy(bf16[64,4096]{1,0:T(8,128)(2,1)} %shard_map.217) | data formatting | bytes 1048576

commit v4 on v3

--- a/solution.py
+++ b/solution.py
@@ -656,27 +656,29 @@
     packed[own_rows, latent_width:] = turn(straight, crossed, cosine[...], sine[...])
     pl.semaphore_wait(barrier, count)
 
-    half = tok // 2
-    mine = lax.rem(tp, 2) * half
-
-    def latent_rows(block, start):
-        return pl.ds(pl.multiple_of(block * tok + start, half), half)
-
-    def latent_out(block):
-        into = packed.at[latent_rows(block, mine)]
-        return remote(into, into, lsend.at[block], lrecv.at[block], {"sp": z + 1})
-
-    def latent_over(block):
-        at = packed.at[latent_rows(block, mine)]
-        return remote(at, at, psend_l.at[block], precv_l.at[block], peer(1))
-
-    def latent_here(block):
-        at = packed.at[latent_rows(block, half - mine)]
-        remote(at, at, psend_l.at[block], precv_l.at[block], peer(1)).wait_recv()
+    pieces = lsend.shape[1]
+    size = tok // (2 * pieces)
+    mine = lax.rem(tp, 2) * pieces
+
+    def latent_rows(block, piece):
+        return packed.at[pl.ds(pl.multiple_of(block * tok + piece * size, size), size)]
+
+    def latent_out(block, k):
+        into = latent_rows(block, mine + k)
+        return remote(into, into, lsend.at[block, k], lrecv.at[block, k], {"sp": z + 1})
+
+    def latent_over(block, k):
+        at = latent_rows(block, mine + k)
+        return remote(at, at, psend_l.at[block, k], precv_l.at[block, k], peer(1))
+
+    def latent_here(block, k):
+        at = latent_rows(block, pieces - mine + k)
+        remote(at, at, psend_l.at[block, k], precv_l.at[block, k], peer(1)).wait_recv()
 
     @pl.when(z < n_sp - 1)
     def _():
-        latent_out(z).start()
+        for k in range(pieces):
+            latent_out(z, k).start()
 
     def fact_out(k):
         return remote(facts_ref, meta.at[me], msend.at[k], mrecv.at[me], other(k))
@@ -725,20 +727,17 @@
 
     def earlier(k, carry):
         block = z - k
-        remote(
-            packed.at[latent_rows(block, mine)],
-            packed.at[latent_rows(block, mine)],
-            lsend.at[block],
-            lrecv.at[block],
-            peer(1),
-        ).wait_recv()
-
-        @pl.when(z < n_sp - 1)
-        def _():
-            latent_out(block).start()
-
-        latent_over(block).start()
-        latent_here(block)
+        for n in range(pieces):
+            at = latent_rows(block, mine + n)
+            remote(at, at, lsend.at[block, n], lrecv.at[block, n], peer(1)).wait_recv()
+
+            @pl.when(z < n_sp - 1)
+            def _():
+                latent_out(block, n).start()
+
+            latent_over(block, n).start()
+        for n in range(pieces):
+            latent_here(block, n)
         attend_rows(block, False)
         return carry
 
@@ -830,6 +829,8 @@
     def staged(*stages):
         def one(q, carry):
             for lag, stage in enumerate(stages):
+                if stage is None:
+                    continue
 
                 @pl.when((q >= lag) & (q < chunks + lag))
                 def _():
@@ -942,9 +943,11 @@
         gather_out(2, q).start()
         gather_out(1, q).start()
 
-    def own_unit(q):
+    def own_relay(q):
         gather_out(2, q).wait_recv()
         gather_on(q).start()
+
+    def own_unit(q):
         gather_out(1, q).wait_recv()
         gather_on(q).wait_recv()
         full = plane[:, cols(q)]
@@ -1035,14 +1038,6 @@
 
         return each
 
-    def at_odd(first):
-        def each(q):
-            @pl.when(lax.rem(q, 2) == 1)
-            def _():
-                own_spread(first + q // 2)
-
-        return each
-
     def sends_done(copies):
         def one(q, carry):
             for copy in copies(q):
@@ -1079,7 +1074,7 @@
 
     for k in (5, 6):
         loads[k].wait()
-    staged(b1, b2, b3, c_first, h_first)
+    staged(b1, b2, b3, None, c_first, None, h_first)
     factor = lax.rsqrt(squares[...] * (1.0 / width) + EPS)
     i, j = grid((rows, factor_out.shape[1]))
     factor = jnp.sum(jnp.where(i == j, factor, 0.0), axis=0, keepdims=True)
@@ -1095,27 +1090,30 @@
         p0, p1, p2 = z + way, z + 2 * way, z + 3 * way
         activate(p0)
         staged(
-            run(lambda q: c_unit(p1, q), down_relay, at_odd(0)),
+            run(lambda q: c_unit(p1, q), down_relay),
+            None,
             run(
+                lambda q: h_unit(p1, q),
                 at_first(lambda: mix_in(p0)),
                 down_ready,
                 lambda q: d_unit(p0, q, False, True, way),
-                lambda q: h_unit(p1, q),
             ),
         )
         activate(p1)
         staged(
-            run(lambda q: c_unit(p2, q), at_odd(chunks // 2)),
+            lambda q: c_unit(p2, q),
+            None,
             run(
+                lambda q: h_unit(p2, q),
                 at_first(lambda: mix_in(p1)),
                 lambda q: d_unit(p1, q, False, False, way),
-                lambda q: h_unit(p2, q),
             ),
         )
         activate(p2)
+        staged(own_spread)
         mix_in(p2)
         staged(lambda q: d_unit(p2, q, False, False, way))
-        staged(own_unit)
+        staged(own_relay, own_unit)
         own_activate()
         staged(rs1, rs2)
         mix_in(z)
@@ -1138,24 +1136,23 @@
         activate(s1)
         staged(
             run(lambda q: c_unit(s2, q, 4, behind), down_relay),
+            None,
             run(lambda q: h_unit(s2, q), down_ready),
         )
+        activate(s2)
         staged(own_spread)
-        activate(s2)
         mix_in(s1)
-        staged(run(own_unit, lambda q: d_unit(s1, q, True, True, way)))
+        mix_in(s0)
+        mix_in(s2)
+        staged(run(own_relay, lambda q: d_unit(s1, q, True, True, way)), own_unit)
         own_activate()
-        mix_in(s2)
-        mix_in(s0)
-        staged(rs1, rs2)
+        staged(
+            run(lambda q: d_unit(s2, q, True, False, way), rs1),
+            rs2,
+            lambda q: d_unit(s0, q, True, True, -way),
+        )
         mix_in(z)
-        staged(
-            run(
-                lambda q: d_unit(s2, q, True, False, way),
-                lambda q: d_unit(s0, q, True, True, -way),
-                base,
-            ),
-        )
+        staged(base)
 
         def last(q):
             total = facc[:, cols(q)] + arrive(0, q) + arrive(1, q)
@@ -1191,11 +1188,13 @@
     def latents_done(block, carry):
         @pl.when(z < n_sp - 1)
         def _():
-            latent_out(block).wait_send()
+            for k in range(pieces):
+                latent_out(block, k).wait_send()
 
         @pl.when(block < z)
         def _():
-            latent_over(block).wait_send()
+            for k in range(pieces):
+                latent_over(block, k).wait_send()
 
         return carry
 
@@ -1254,7 +1253,7 @@
     scratch += [half(n_sp, n_tp, rows, hidden)]
     scratch += [full(n_tp * rows, share)] * 2 + [half(n_tp * rows, share)]
     scratch += [full(rows, width), full(rows, 1)]
-    scratch += [sems(10)] + [sems(n_sp)] * 4
+    scratch += [sems(10)] + [sems(n_sp, 2)] * 4
     scratch += [sems(count)] * 4
     scratch += [sems(n_tp, chunks)] * 2
     scratch += [sems(5, chunks), sems(n_sp, chunks)]

time: 122 us -> 115 us (0.943)
  Pallas kernels: 120 us -> 113 us
    pallas_call x1, Pallas kernels: 120 us -> 113 us  [layer(): pl.pallas_call(lambda *refs: layer_kernel(chunks, cap, sizes, *refs), out...]
where the time goes in v4:
time: 115 us
  Pallas kernels  113 us (98%)
  local copies, waits for them, and re-layouts  1.87 us (2%)
    pallas_call x1, Pallas kernels, layer(): pl.pallas_call(lambda *refs: layer_kernel(chunks, cap, sizes, *refs), out...  113 us

profile of v4, /device:TPU:0, one launch (start us, length us, event | category | flops | bytes accessed | tf_op | source)
XLA Modules:
  0.0 115.1 jit_solution(2370082810537405670)
XLA Ops:
  0.0 113.2 %shard_map.217 = bf16[64,4096]{1,0:T(8,128)(2,1)} custom-call(bf16[256,512]{1,0:T(8,128)(2,1)} %refs_0_.1, bf16[64,256]{1,0:T(8,128)(2,1)} %bitcast.15, f32[1,512]{1,0:T(1,128)} %bitcast.17, bf16[256,384]{1,0:T(8,128)(2,1)} %refs_3_.1, bf16[256,256]{1,0:T(8,128)(2,1)} %refs_4_.1, bf16[512,256]{1,0:T(8,128)(2,1)} %refs_5_.1, bf16[512,128]{1,0:T(8,128)(2,1)} %refs_6_.1, ...), custom_call_target="tpu_custom_call" | custom-call | tf_op jit(solution)/shard_map/pallas_call | solution.py:1264
  113.2 1.9 %copy.25 = bf16[64,4096]{1,0:T(8,128)(2,1)} copy(bf16[64,4096]{1,0:T(8,128)(2,1)} %shard_map.217) | data formatting | bytes 1048576

commit v5 on v4

--- a/solution.py
+++ b/solution.py
@@ -821,10 +821,22 @@
 
         plane[:rows, cols(q)] = scaled
 
+        @pl.when(q == chunks - 1)
+        def _():
+            send_factor()
+
         @pl.when(q < chunks // 2)
         def _():
             down_out(2, 2 * q + group).wait_recv()
             down_across(2 * q + group).start()
+
+    def send_factor():
+        factor = lax.rsqrt(squares[...] * (1.0 / width) + EPS)
+        i, j = grid((rows, factor_out.shape[1]))
+        factor = jnp.sum(jnp.where(i == j, factor, 0.0), axis=0, keepdims=True)
+        factor_out[...] = jnp.broadcast_to(factor, factor_out.shape)
+        others(lambda k: factor_send(k).start())
+        factors[me] = factor_out[...]
 
     def staged(*stages):
         def one(q, carry):
@@ -1038,6 +1050,21 @@
 
         return each
 
+    def at_last(step):
+        def each(q):
+            @pl.when(q == chunks - 1)
+            def _():
+                step()
+
+        return each
+
+    def spread_some(first, stop):
+        def step():
+            for k in range(first, stop):
+                own_spread(k)
+
+        return step
+
     def sends_done(copies):
         def one(q, carry):
             for copy in copies(q):
@@ -1075,12 +1102,6 @@
     for k in (5, 6):
         loads[k].wait()
     staged(b1, b2, b3, None, c_first, None, h_first)
-    factor = lax.rsqrt(squares[...] * (1.0 / width) + EPS)
-    i, j = grid((rows, factor_out.shape[1]))
-    factor = jnp.sum(jnp.where(i == j, factor, 0.0), axis=0, keepdims=True)
-    factor_out[...] = jnp.broadcast_to(factor, factor_out.shape)
-    others(lambda k: factor_send(k).start())
-    factors[me] = factor_out[...]
 
     for k in (2, 3, 4):
         loads[k].wait()
@@ -1088,10 +1109,9 @@
     @pl.when(is_end)
     def _():
         p0, p1, p2 = z + way, z + 2 * way, z + 3 * way
-        activate(p0)
         staged(
-            run(lambda q: c_unit(p1, q), down_relay),
-            None,
+            run(lambda q: c_unit(p1, q), down_relay, at_last(spread_some(0, chunks // 4))),
+            at_first(lambda: activate(p0)),
             run(
                 lambda q: h_unit(p1, q),
                 at_first(lambda: mix_in(p0)),
@@ -1099,10 +1119,9 @@
                 lambda q: d_unit(p0, q, False, True, way),
             ),
         )
-        activate(p1)
         staged(
             lambda q: c_unit(p2, q),
-            None,
+            at_first(lambda: activate(p1)),
             run(
                 lambda q: h_unit(p2, q),
                 at_first(lambda: mix_in(p1)),
@@ -1110,7 +1129,7 @@
             ),
         )
         activate(p2)
-        staged(own_spread)
+        spread_some(chunks // 4, chunks)()
         mix_in(p2)
         staged(lambda q: d_unit(p2, q, False, False, way))
         staged(own_relay, own_unit)
@@ -1132,11 +1151,9 @@
     @pl.when(jnp.logical_not(is_end))
     def _():
         s0, s1, s2 = z - way, z + way, z + 2 * way
-        activate(s0)
-        activate(s1)
         staged(
             run(lambda q: c_unit(s2, q, 4, behind), down_relay),
-            None,
+            run(at_first(lambda: activate(s0)), at_first(lambda: activate(s1))),
             run(lambda q: h_unit(s2, q), down_ready),
         )
         activate(s2)

time: 115 us -> 111 us (0.965)
  Pallas kernels: 113 us -> 109 us
    pallas_call x1, Pallas kernels: 113 us -> 109 us  [layer(): pl.pallas_call(lambda *refs: layer_kernel(chunks, cap, sizes, *refs), out...]
where the time goes in v5:
time: 111 us
  Pallas kernels  109 us (98%)
  local copies, waits for them, and re-layouts  1.87 us (2%)
    pallas_call x1, Pallas kernels, layer(): pl.pallas_call(lambda *refs: layer_kernel(chunks, cap, sizes, *refs), out...  109 us

profile of v5, /device:TPU:0, one launch (start us, length us, event | category | flops | bytes accessed | tf_op | source)
XLA Modules:
  0.0 111.3 jit_solution(60257230513288929)
XLA Ops:
  0.0 109.4 %shard_map.217 = bf16[64,4096]{1,0:T(8,128)(2,1)} custom-call(bf16[256,512]{1,0:T(8,128)(2,1)} %refs_0_.1, bf16[64,256]{1,0:T(8,128)(2,1)} %bitcast.15, f32[1,512]{1,0:T(1,128)} %bitcast.17, bf16[256,384]{1,0:T(8,128)(2,1)} %refs_3_.1, bf16[256,256]{1,0:T(8,128)(2,1)} %refs_4_.1, bf16[512,256]{1,0:T(8,128)(2,1)} %refs_5_.1, bf16[512,128]{1,0:T(8,128)(2,1)} %refs_6_.1, ...), custom_call_target="tpu_custom_call" | custom-call | tf_op jit(solution)/shard_map/pallas_call | solution.py:1281
  109.4 1.9 %copy.25 = bf16[64,4096]{1,0:T(8,128)(2,1)} copy(bf16[64,4096]{1,0:T(8,128)(2,1)} %shard_map.217) | data formatting | bytes 1048576
